TPU v7x, 32 devices: a whole 2x2x4 slice. The times are simulated.
32 devices in a mesh: ep: 8 (over z, core), tp: 4 (over y, x).
Axes of the slice: x: 2, y: 2, z: 4, core: 2. Of those that a mesh axis runs over, the one named last changes fastest.
Arguments:
- query_rows: bfloat16 [4096, 2048], P('ep', 'tp'), may hold values from -6 to 6
- key_rows: bfloat16 [4096, 2048], P('ep', 'tp'), may hold values from -6 to 6
- value_rows: bfloat16 [4096, 4096], P('ep', 'tp'), may hold values from -6 to 6
- in_gate: float32 [16, 4096], P('tp', 'ep'), may hold values from -120 to 120
- forget_gate: float32 [16, 4096], P('tp', 'ep'), may hold values from -2 to 20
- out_gate: bfloat16 [4096, 4096], P('ep', 'tp'), may hold values from -6 to 6
- head_gain: float32 [4096], P('tp'), may hold values from 0.1 to 1.9
- mix_weight: bfloat16 [4096, 4096], P(None, 'tp'), may hold values from -0.09375 to 0.09375
- expert_input: bfloat16 [2048, 4096], P('ep', 'tp'), may hold values from -30 to 30
- routes: int32 [2048, 2], P('ep'), may hold values from 0 to 7, all different within a row; in each aligned block of 256 rows (0 to 255, 256 to 511, ...) at most 128 rows name the same one
- route_weight: float32 [2048, 2], P('ep'), may hold values from 0.25 to 1.25
- gate_weight: bfloat16 [8, 1024, 4096], P('ep', 'tp'), may hold values from -0.09375 to 0.09375
- up_weight: bfloat16 [8, 1024, 4096], P('ep', 'tp'), may hold values from -0.09375 to 0.09375
- down_weight: bfloat16 [8, 1024, 4096], P('ep', None, 'tp'), may hold values from -0.1875 to 0.1875
Outputs:
- mixer_out: bfloat16 [4096, 4096], P('ep', 'tp')
- expert_out: bfloat16 [2048, 4096], P('ep', 'tp')
Inputs may be any that keep to these rules, and one draw needn't show every extreme that they name: `routes`: each row names 2 different experts. In the rows of one device no expert is named by more than 128 rows, and in the rows of some device an expert is named by exactly 128 rows.
All inputs are finite; a program needn't handle non-finite values.
Results may differ from a plain program's by a relative error of at most 0.0057.
Values may be sent and summed in bfloat16 or wider, within the bound.
A program may use at most 128 MiB of HBM per device.

v0:
```python
import functools

import jax
import jax.numpy as jnp
from jax import lax
from jax.experimental import pallas as pl
from jax.experimental.pallas import tpu as pltpu
from jax.sharding import PartitionSpec as P

EPSILON = 1e-06
LOG_FLOOR = -1e30
F32 = jnp.float32
BF16 = jnp.bfloat16
GROUPS = 4
PAD = 16


def flip(index, bits):
    place = 1
    while place <= bits:
        if bits & place:
            index = index + place * (1 - 2 * ((index // place) % 2))
        place *= 2
    return index


def dot(left, right, contract=((1,), (0,))):
    return lax.dot_general(left, right, (contract, ((), ())), preferred_element_type=F32)


def upright(row):
    size = row.shape[1]
    own = lax.broadcasted_iota(jnp.int32, (size, size), 0) == lax.broadcasted_iota(
        jnp.int32, (size, size), 1
    )
    return jnp.sum(jnp.where(own, row, jnp.zeros((), row.dtype)), axis=1, keepdims=True)


def kernel(
    ep,
    tp,
    head_count,
    model_width,
    x_ref,
    slot_row_ref,
    weight_ref,
    a_ref,
    cum_ref,
    gain_ref,
    q_hbm,
    k_hbm,
    v_hbm,
    og_hbm,
    wg_hbm,
    wu_hbm,
    wd_hbm,
    wm_hbm,
    mix_ref,
    exp_ref,
    q_ref,
    k_ref,
    v_ref,
    og_ref,
    wg_ref,
    wu_ref,
    wd_ref,
    wm_ref,
    slots,
    tok,
    hid,
    outb,
    ret,
    hm,
    local,
    st_in,
    st_out,
    load_sem,
    disp_send,
    disp_recv,
    tok_send,
    tok_recv,
    fwd_send,
    fwd_recv,
    hid_send,
    hid_recv,
    ret_send,
    ret_recv,
    head_send,
    head_recv,
    hfwd_send,
    hfwd_recv,
    st_send,
    st_recv,
):
    me = lax.axis_index("ep")
    mine = lax.axis_index("tp")
    cap = slots.shape[0] // ep
    span = slots.shape[0] // GROUPS
    per = ep // GROUPS
    width = x_ref.shape[1]
    length = q_ref.shape[0]
    qk = q_ref.shape[1] // head_count
    vw = v_ref.shape[1] // head_count
    units = wg_ref.shape[0]
    square = tp == 4

    loads = [
        pltpu.make_async_copy(source, target, load_sem.at[at])
        for at, (source, target) in enumerate(
            [
                (k_hbm, k_ref),
                (v_hbm, v_ref),
                (q_hbm, q_ref),
                (og_hbm, og_ref),
                (wg_hbm, wg_ref),
                (wu_hbm, wu_ref),
                (wd_hbm, wd_ref),
                (wm_hbm, wm_ref),
            ]
        )
    ]
    for load in loads:
        load.start()

    barrier = pltpu.get_barrier_semaphore()
    for i in range(1, ep):
        pl.semaphore_signal(barrier, inc=1, device_id={"ep": flip(me, i)})
    for j in range(1, tp):
        pl.semaphore_signal(barrier, inc=1, device_id={"tp": flip(mine, j)})

    tokens = x_ref.shape[0]

    def pick(group, carry):
        at = group * span
        rows = at + lax.broadcasted_iota(jnp.int32, (span, tokens), 0)
        hit = (rows == slot_row_ref[0:1, :]) | (rows == slot_row_ref[1:2, :])
        chosen = dot(hit.astype(F32).astype(BF16), x_ref[...]).astype(BF16)
        slots[pl.ds(pl.multiple_of(at, span), span), :] = chosen
        return carry

    lax.fori_loop(0, GROUPS, pick, 0)
    pl.semaphore_wait(barrier, ep - 1 + tp - 1)

    def dispatch(i):
        return pltpu.make_async_remote_copy(
            slots.at[pl.ds(i * cap, cap)],
            tok.at[0, pl.ds(i * cap, cap)],
            disp_send.at[i],
            disp_recv.at[i],
            device_id={"ep": flip(me, i)},
        )

    near = max(2, 2 * per)
    waits_for_chain = me % 2 == 1
    for i in range(1, ep):
        if i < near:
            dispatch(i).start()
        else:
            held = waits_for_chain & (flip(me, i) > me)

            @pl.when(jnp.logical_not(held))
            def _():
                dispatch(i).start()

    tok[0, 0:cap, :] = slots[0:cap, :]

    def spread(group, j):
        return pltpu.make_async_remote_copy(
            tok.at[0, pl.ds(group * span, span)],
            tok.at[j, pl.ds(group * span, span)],
            tok_send.at[group, j],
            tok_recv.at[group, j],
            device_id={"tp": flip(mine, j)},
        )

    half = span // 2

    def onward(group, j):
        part = pl.ds(group * span + (j - 1) * half, half)
        return pltpu.make_async_remote_copy(
            tok.at[j, part],
            tok.at[3, part],
            fwd_send.at[group, j],
            fwd_recv.at[group, j],
            device_id={"tp": flip(mine, 3 - j)},
        )

    direct = (1, 2) if square else tuple(range(1, tp))

    def send_group(group):
        for i in range(max(1, group * per), (group + 1) * per):
            dispatch(i).wait_recv()
        for j in direct:
            spread(group, j).start()

    def relay_group(group):
        if square:
            for j in (1, 2):
                spread(group, j).wait_recv()
                onward(group, j).start()

    def collect_group(group):
        if square:
            for j in (1, 2):
                onward(group, j).wait_recv()
        else:
            for j in direct:
                spread(group, j).wait_recv()

    send_group(0)

    loads[0].wait()
    loads[1].wait()

    def summarise(h, carry):
        keys = k_ref[:, pl.ds(pl.multiple_of(h * qk, qk), qk)]
        values = v_ref[:, pl.ds(pl.multiple_of(h * vw, vw), vw)]
        log_in = a_ref[pl.ds(h, 1), :]
        top = jnp.max(log_in, axis=1, keepdims=True)
        weighted = keys.astype(F32) * jnp.exp(upright(log_in) - top)
        local[h, 0:qk, :] = dot(weighted.astype(BF16), values, ((0,), (0,)))
        normal = jnp.sum(weighted, axis=0, keepdims=True)
        local[h, qk : qk + 8, 0:qk] = jnp.broadcast_to(normal, (8, qk))
        decay = cum_ref[pl.ds(h, 1), :][:, length - 1 : length]
        local[h, qk + 8 : qk + 16, :] = jnp.broadcast_to(top + decay, (8, vw))
        return carry

    lax.fori_loop(0, head_count, summarise, 0)

    @pl.when(me >= ep // 2)
    def _():
        send_group(1)
        relay_group(0)

    def chain(h):
        return pltpu.make_async_remote_copy(
            st_out.at[h],
            st_in.at[h],
            st_send.at[h],
            st_recv.at[h],
            device_id={"ep": me + 1},
        )

    @pl.when(me == 0)
    def _():
        st_in[:, 0 : qk + 8, :] = jnp.zeros((head_count, qk + 8, vw), F32)
        st_in[:, qk + 8 : qk + 16, :] = jnp.full((head_count, 8, vw), LOG_FLOOR, F32)

    for h in range(head_count):

        @pl.when(me > 0)
        def _():
            chain(h).wait_recv()

        decay = cum_ref[h : h + 1, length - 1 : length]
        carried_max = st_in[h, qk + 8 : qk + 9, :] + decay
        own_max = local[h, qk + 8 : qk + 9, :]
        new_max = jnp.maximum(carried_max, own_max)
        keep = jnp.exp(carried_max - new_max)
        add = jnp.exp(own_max - new_max)
        st_out[h, 0:qk, :] = keep * st_in[h, 0:qk, :] + add * local[h, 0:qk, :]
        st_out[h, qk : qk + 8, 0:qk] = (
            keep[:, 0:qk] * st_in[h, qk : qk + 8, 0:qk]
            + add[:, 0:qk] * local[h, qk : qk + 8, 0:qk]
        )
        st_out[h, qk : qk + 8, qk:vw] = jnp.zeros((8, vw - qk), F32)
        st_out[h, qk + 8 : qk + 16, :] = jnp.broadcast_to(new_max, (8, vw))

        @pl.when(me < ep - 1)
        def _():
            chain(h).start()

    for i in range(near, ep):
        held = waits_for_chain & (flip(me, i) > me)

        @pl.when(held)
        def _():
            dispatch(i).start()

    @pl.when(me < ep // 2)
    def _():
        send_group(1)
        relay_group(0)

    loads[2].wait()
    loads[3].wait()

    def heads(h, carry):
        columns = pl.ds(pl.multiple_of(h * vw, vw), vw)
        queries = q_ref[:, pl.ds(pl.multiple_of(h * qk, qk), qk)]
        keys = k_ref[:, pl.ds(pl.multiple_of(h * qk, qk), qk)]
        scale = qk**-0.5
        causal = lax.broadcasted_iota(jnp.int32, (length, length), 1) <= lax.broadcasted_iota(
            jnp.int32, (length, length), 0
        )
        log_in = jnp.where(causal, a_ref[pl.ds(h, 1), :], -jnp.inf)
        prior_max = st_in[h, qk + 8 : qk + 9, 0:1]
        top = jnp.maximum(prior_max, jnp.max(log_in, axis=1, keepdims=True))
        scores = dot(queries, keys, ((1,), (1,))) * scale * jnp.exp(log_in - top)
        carried = jnp.exp(prior_max - top) * scale
        memory = st_in[h, 0:qk, :]
        high = memory.astype(BF16)
        low = (memory - high.astype(F32)).astype(BF16)
        numerator = carried * (dot(queries, high) + dot(queries, low)) + dot(
            scores.astype(BF16), v_ref[:, columns]
        )
        normal = st_in[h, qk : qk + 1, 0:qk]
        denominator = carried * jnp.sum(
            queries.astype(F32) * normal, axis=1, keepdims=True
        ) + jnp.sum(scores, axis=1, keepdims=True)
        floor = jnp.exp(-(upright(cum_ref[pl.ds(h, 1), :]) + top))
        value = numerator / jnp.maximum(jnp.abs(denominator), floor)
        value = value * lax.rsqrt(jnp.mean(value * value, axis=1, keepdims=True) + EPSILON)
        gate = jax.nn.sigmoid(og_ref[:, columns].astype(F32))
        hm[0, :, columns] = (value * gain_ref[:, columns] * gate).astype(BF16)
        return carry

    lax.fori_loop(0, head_count // 2, heads, 0)
    relay_group(1)
    send_group(2)
    lax.fori_loop(head_count // 2, head_count, heads, 0)

    loads[4].wait()
    loads[5].wait()

    def expand(group):
        rows = pl.ds(group * span, span)

        gate = jnp.zeros((span, units), F32)
        up = jnp.zeros((span, units), F32)
        squares = jnp.zeros((span, 1), F32)
        for j in range(tp):
            piece = tok[j, rows, :]
            columns = pl.ds(pl.multiple_of(flip(mine, j) * width, width), width)
            gate += dot(piece, wg_ref[:, columns], ((1,), (1,)))
            up += dot(piece, wu_ref[:, columns], ((1,), (1,)))
            wide = piece.astype(F32)
            squares += jnp.sum(wide * wide, axis=1, keepdims=True)
        inverse = lax.rsqrt(squares / model_width + EPSILON)
        hid[0, rows, :] = (jax.nn.silu(gate * inverse) * (up * inverse)).astype(BF16)

    def share(group, j):
        return pltpu.make_async_remote_copy(
            hid.at[0, pl.ds(group * span, span)],
            hid.at[j, pl.ds(group * span, span)],
            hid_send.at[group, j],
            hid_recv.at[group, j],
            device_id={"tp": flip(mine, j)},
        )

    def give_back(i):
        return pltpu.make_async_remote_copy(
            outb.at[pl.ds(i * cap, cap)],
            ret.at[pl.ds(i * cap, cap)],
            ret_send.at[i],
            ret_recv.at[i],
            device_id={"ep": flip(me, i)},
        )

    def contract(group):
        rows = pl.ds(group * span, span)
        for j in range(1, tp):
            share(group, j).wait_recv()
        total = jnp.zeros((span, width), F32)
        for j in range(tp):
            at = pl.ds(pl.multiple_of(flip(mine, j) * units, units), units)
            total += dot(hid[j, rows, :], wd_ref[at, :])
        outb[rows, :] = total.astype(BF16)
        for i in range(max(1, group * per), (group + 1) * per):
            give_back(i).start()

    tile = length // 2

    def head_spread(part, j):
        rows = pl.ds(part * tile, tile)
        return pltpu.make_async_remote_copy(
            hm.at[0, rows],
            hm.at[j, rows],
            head_send.at[part, j],
            head_recv.at[part, j],
            device_id={"tp": flip(mine, j)},
        )

    def head_onward(part, j):
        rows = pl.ds(part * tile + (j - 1) * (tile // 2), tile // 2)
        return pltpu.make_async_remote_copy(
            hm.at[j, rows],
            hm.at[3, rows],
            hfwd_send.at[part, j],
            hfwd_recv.at[part, j],
            device_id={"tp": flip(mine, 3 - j)},
        )

    def expand_and_share(group):
        collect_group(group)
        expand(group)
        for j in range(1, tp):
            share(group, j).start()

    loads[6].wait()
    for group in range(GROUPS):
        if group > 1:
            if group + 1 < GROUPS:
                relay_group(group + 1)
        expand_and_share(group)
        if group == 0:
            for later in range(3, GROUPS):
                send_group(later)
            relay_group(2)
        elif group < GROUPS - 1:
            contract(group - 1)
    for part in range(2):
        for j in direct:
            head_spread(part, j).start()
    contract(GROUPS - 2)
    contract(GROUPS - 1)
    ret[0:cap, :] = outb[0:cap, :]

    loads[7].wait()
    if square:
        for part in range(2):
            for j in (1, 2):
                head_spread(part, j).wait_recv()
                head_onward(part, j).start()

    def mix(part):
        rows = pl.ds(part * tile, tile)
        for j in range(1, tp):
            if not square:
                head_spread(part, j).wait_recv()
            elif j < 3:
                head_onward(part, j).wait_recv()
        total = jnp.zeros((tile, width), F32)
        for j in range(tp):
            inputs = pl.ds(pl.multiple_of(flip(mine, j) * width, width), width)
            total += dot(hm[j, rows, :], wm_ref[inputs, :])
        mix_ref[rows, :] = total.astype(BF16)

    mix(0)

    for i in range(1, ep):
        give_back(i).wait_recv()
    places = lax.broadcasted_iota(jnp.int32, (slots.shape[0], tokens), 0)
    total = jnp.zeros((tokens, width), F32)
    for route in range(weight_ref.shape[0]):
        hit = places == slot_row_ref[route : route + 1, :]
        picked = dot(hit.astype(F32).astype(BF16), ret[...], ((0,), (0,)))
        total += picked * upright(weight_ref[route : route + 1, :])
    exp_ref[...] = total.astype(BF16)

    mix(1)

    for i in range(1, ep):
        dispatch(i).wait_send()
        give_back(i).wait_send()
    for group in range(GROUPS):
        for j in direct:
            spread(group, j).wait_send()
        for j in range(1, tp):
            share(group, j).wait_send()
        if square:
            for j in (1, 2):
                onward(group, j).wait_send()
    for part in range(2):
        for j in direct:
            head_spread(part, j).wait_send()
        if square:
            for j in (1, 2):
                head_onward(part, j).wait_send()
    for h in range(head_count):

        @pl.when(me < ep - 1)
        def _():
            chain(h).wait_send()


def body(
    query_rows,
    key_rows,
    value_rows,
    in_gate,
    forget_gate,
    out_gate,
    head_gain,
    mix_weight,
    expert_input,
    routes,
    route_weight,
    gate_weight,
    up_weight,
    down_weight,
):
    ep, tp = lax.axis_size("ep"), lax.axis_size("tp")
    head_count, length = in_gate.shape
    token_count, fanout = routes.shape
    width = expert_input.shape[1]
    units = gate_weight.shape[1]
    capacity = 2 * token_count * fanout // ep
    slot_count = ep * capacity
    qk = query_rows.shape[1] // head_count
    vw = value_rows.shape[1] // head_count

    earlier = jnp.tril(jnp.ones((length, length), F32))
    cumulative = jnp.einsum(
        "hs,ts->ht", jax.nn.log_sigmoid(forget_gate), earlier, precision=lax.Precision.HIGHEST
    )
    shifted = in_gate - cumulative

    me = lax.axis_index("ep")
    turned = routes ^ me
    experts = jnp.arange(ep, dtype=jnp.int32)
    named = turned[:, :, None] == experts
    any_named = jnp.any(named, axis=1)
    before = jnp.dot(
        jnp.tril(jnp.ones((token_count, token_count), BF16), -1),
        any_named.astype(BF16),
        preferred_element_type=F32,
    ).astype(jnp.int32)
    places = experts * capacity + before
    slot_row = jnp.sum(jnp.where(named, places[:, None, :], 0), axis=2).T

    vmem = pl.BlockSpec(memory_space=pltpu.VMEM)
    anywhere = pl.BlockSpec(memory_space=pl.ANY)
    dma = pltpu.SemaphoreType.DMA
    gate_local, up_local, down_local = gate_weight[0], up_weight[0], down_weight[0]
    big = (query_rows, key_rows, value_rows, out_gate, gate_local, up_local, down_local, mix_weight)
    state = (head_count, qk + PAD, vw)
    return pl.pallas_call(
        functools.partial(kernel, ep, tp, head_count, mix_weight.shape[0]),
        out_shape=(
            jax.ShapeDtypeStruct((length, width), BF16),
            jax.ShapeDtypeStruct((token_count, width), BF16),
        ),
        in_specs=[vmem] * 6 + [anywhere] * 8,
        out_specs=(vmem, vmem),
        scratch_shapes=[pltpu.VMEM(array.shape, array.dtype) for array in big]
        + [
            pltpu.VMEM((slot_count, width), BF16),
            pltpu.VMEM((tp, slot_count, width), BF16),
            pltpu.VMEM((tp, slot_count, units), BF16),
            pltpu.VMEM((slot_count, width), BF16),
            pltpu.VMEM((slot_count, width), BF16),
            pltpu.VMEM((tp, length, width), BF16),
            pltpu.VMEM(state, F32),
            pltpu.VMEM(state, F32),
            pltpu.VMEM(state, F32),
            dma((8,)),
            dma((ep,)),
            dma((ep,)),
            dma((GROUPS, tp)),
            dma((GROUPS, tp)),
            dma((GROUPS, 4)),
            dma((GROUPS, 4)),
            dma((GROUPS, tp)),
            dma((GROUPS, tp)),
            dma((ep,)),
            dma((ep,)),
            dma((2, tp)),
            dma((2, tp)),
            dma((2, 4)),
            dma((2, 4)),
            dma((head_count,)),
            dma((head_count,)),
        ],
        compiler_params=pltpu.CompilerParams(
            collective_id=0, has_side_effects=True, vmem_limit_bytes=64000 * 1024
        ),
    )(
        expert_input,
        slot_row,
        route_weight.T,
        shifted,
        cumulative,
        head_gain[None, :],
        *big,
    )


def solution(mesh):
    in_specs = (
        P("ep", "tp"),
        P("ep", "tp"),
        P("ep", "tp"),
        P("tp", "ep"),
        P("tp", "ep"),
        P("ep", "tp"),
        P("tp"),
        P(None, "tp"),
        P("ep", "tp"),
        P("ep", None),
        P("ep", None),
        P("ep", "tp", None),
        P("ep", "tp", None),
        P("ep", None, "tp"),
    )
    out_specs = (P("ep", "tp"), P("ep", "tp"))
    return jax.shard_map(body, mesh=mesh, in_specs=in_specs, out_specs=out_specs, check_vma=False)
```

profile of v0, /device:TPU:8, one launch (start us, length us, event | category | flops | bytes accessed | tf_op | source)
XLA Modules:
  0.0 173.2 jit_solution(6788261632074362285)
XLA Ops:
  0.7 0.7 broadcast_xor_fusion
  1.4 0.2 fusion
  1.6 0.6 select_reduce_fusion
  2.2 2.0 %fusion.25 = (f32[4,512]{1,0:T(4,128)}, f32[4,512]{1,0:T(4,128)}) fusion(f32[4,512]{1,0:T(4,128)} %param.17, f32[4,512]{1,0:T(4,128)} %param.18), kind=kOutput, calls=%fused_computation.32 | convolution fusion | flops 13125632 | bytes 32768 | tf_op jit(solution)/shard_map/hs,ts->ht/dot_general | solution.py:504
  4.2 165.9 %shard_map.149 = (bf16[512,1024]{1,0:T(8,128)(2,1)}, bf16[256,1024]{1,0:T(8,128)(2,1)}) custom-call(bf16[256,1024]{1,0:T(8,128)(2,1)} %x_ref.1, s32[2,256]{1,0:T(2,128)} %bitcast.10, f32[2,256]{1,0:T(2,128)} %bitcast.12, f32[4,512]{1,0:T(4,128)} %get-tuple-element.2.a_ref, f32[4,512]{1,0:T(4,128)} %get-tuple-element.3.cum_ref, f32[1,1024]{1,0:T(1,128)} %bitcast.11, ...), custom_call_target="tpu_custom_call" | custom-call | tf_op jit(solution)/shard_map/pallas_call | solution.py:528
  170.1 0.0 copy-start
  170.1 2.3 %copy.20 = bf16[512,1024]{1,0:T(8,128)(2,1)} copy(bf16[512,1024]{1,0:T(8,128)(2,1)} %get-tuple-element.6) | data formatting | bytes 2097152
  172.5 0.0 copy-done
  172.5 0.8 copy.21
  (3 shorter events, 0.0 us)
Async XLA Ops:
  170.1 2.3 %copy-start = (bf16[256,1024]{1,0:T(8,128)(2,1)S(1)}, bf16[256,1024]{1,0:T(8,128)(2,1)}, u32[]{:S(2)}) copy-start(bf16[256,1024]{1,0:T(8,128)(2,1)} %get-tuple-element.7) | copy-start | bytes 1572868
where the time goes:
time: 174 us; the launch traced here: 173 us
  Pallas kernels  166 us (95%)
  local copies, waits for them, and re-layouts  3.12 us (2%)
  matrix products  2.21 us (1%)
    pallas_call x1, Pallas kernels, body(): pl.pallas_call(functools.partial(kernel, ep, tp, head_count, mix_weight.s...  166 us

commit v1 on v0

v1 whole, which is shorter than its diff:
```python
import functools

import jax
import jax.numpy as jnp
from jax import lax
from jax.experimental import pallas as pl
from jax.experimental.pallas import tpu as pltpu
from jax.sharding import PartitionSpec as P

EPSILON = 1e-06
LOG_FLOOR = -1e30
F32 = jnp.float32
BF16 = jnp.bfloat16
GROUPS = 8
PARTS = 4
PAD = 16


def flip(index, bits):
    place = 1
    while place <= bits:
        if bits & place:
            index = index + place * (1 - 2 * ((index // place) % 2))
        place *= 2
    return index


def flip_by(index, bits, size):
    place = 1
    while place < size:
        index = index + ((bits // place) % 2) * place * (1 - 2 * ((index // place) % 2))
        place *= 2
    return index


def dot(left, right, contract=((1,), (0,))):
    return lax.dot_general(left, right, (contract, ((), ())), preferred_element_type=F32)


def upright(row):
    size = row.shape[1]
    own = lax.broadcasted_iota(jnp.int32, (size, size), 0) == lax.broadcasted_iota(
        jnp.int32, (size, size), 1
    )
    return jnp.sum(jnp.where(own, row, jnp.zeros((), row.dtype)), axis=1, keepdims=True)


def scope(name):
    return jax.named_scope(name)


def kernel(
    ep,
    tp,
    head_count,
    model_width,
    x_ref,
    slot_row_ref,
    weight_ref,
    a_ref,
    cum_ref,
    gain_ref,
    q_hbm,
    k_hbm,
    v_hbm,
    og_hbm,
    wg_hbm,
    wu_hbm,
    wd_hbm,
    wm_hbm,
    mix_ref,
    exp_ref,
    q_ref,
    k_ref,
    v_ref,
    og_ref,
    wg_ref,
    wu_ref,
    wd_ref,
    wm_ref,
    slots,
    tok,
    hid,
    outb,
    ret,
    hm,
    local,
    st_in,
    st_out,
    load_sem,
    disp_send,
    disp_recv,
    tok_send,
    tok_recv,
    fwd_send,
    fwd_recv,
    hid_send,
    hid_recv,
    hidf_send,
    hidf_recv,
    ret_send,
    ret_recv,
    head_send,
    head_recv,
    hfwd_send,
    hfwd_recv,
    st_send,
    st_recv,
):
    me = lax.axis_index("ep")
    mine = lax.axis_index("tp")
    cap = slots.shape[0] // ep
    span = slots.shape[0] // GROUPS
    per = ep // GROUPS
    width = x_ref.shape[1]
    length = q_ref.shape[0]
    qk = q_ref.shape[1] // head_count
    vw = v_ref.shape[1] // head_count
    units = wg_ref.shape[0]
    square = tp == 4
    direct = (1, 2) if square else tuple(range(1, tp))

    loads = [
        pltpu.make_async_copy(source, target, load_sem.at[at])
        for at, (source, target) in enumerate(
            [
                (k_hbm, k_ref),
                (v_hbm, v_ref),
                (q_hbm, q_ref),
                (og_hbm, og_ref),
                (wg_hbm, wg_ref),
                (wu_hbm, wu_ref),
                (wd_hbm, wd_ref),
                (wm_hbm, wm_ref),
            ]
        )
    ]
    for load in loads:
        load.start()

    barrier = pltpu.get_barrier_semaphore()
    for i in range(1, ep):
        pl.semaphore_signal(barrier, inc=1, device_id={"ep": flip(me, i)})
    for j in range(1, tp):
        pl.semaphore_signal(barrier, inc=1, device_id={"tp": flip(mine, j)})

    tokens = x_ref.shape[0]

    def block(at, size):
        return pl.ds(pl.multiple_of(at * size, size), size)

    def pick(part, carry):
        size = slots.shape[0] // 4
        rows = part * size + lax.broadcasted_iota(jnp.int32, (size, tokens), 0)
        hit = (rows == slot_row_ref[0:1, :]) | (rows == slot_row_ref[1:2, :])
        chosen = dot(hit.astype(F32).astype(BF16), x_ref[...]).astype(BF16)
        slots[block(part, size), :] = chosen
        return carry

    with scope("pick"):
        lax.fori_loop(0, 4, pick, 0)
    tok[0, 0:cap, :] = slots[0:cap, :]
    with scope("barrier"):
        pl.semaphore_wait(barrier, ep - 1 + tp - 1)

    def dispatch(i):
        return pltpu.make_async_remote_copy(
            slots.at[block(i, cap)],
            tok.at[0, block(i, cap)],
            disp_send.at[i],
            disp_recv.at[i],
            device_id={"ep": flip_by(me, i, ep)},
        )

    def held(i):
        ahead = (me % 2 == 1) & (flip(me, i) > me)
        return ahead if i >= ep // 2 else ahead & (me < 2)

    def spread(group, j):
        return pltpu.make_async_remote_copy(
            tok.at[0, block(group, span)],
            tok.at[j, block(group, span)],
            tok_send.at[group, j],
            tok_recv.at[group, j],
            device_id={"tp": flip(mine, j)},
        )

    half = span // 2

    def onward(group, j):
        part = pl.ds(pl.multiple_of(group * span + (j - 1) * half, half), half)
        return pltpu.make_async_remote_copy(
            tok.at[j, part],
            tok.at[3, part],
            fwd_send.at[group, j],
            fwd_recv.at[group, j],
            device_id={"tp": flip(mine, 3 - j)},
        )

    def share(group, j):
        return pltpu.make_async_remote_copy(
            hid.at[0, block(group, span)],
            hid.at[j, block(group, span)],
            hid_send.at[group, j],
            hid_recv.at[group, j],
            device_id={"tp": flip(mine, j)},
        )

    def share_onward(group, j):
        part = pl.ds(pl.multiple_of(group * span + (j - 1) * half, half), half)
        return pltpu.make_async_remote_copy(
            hid.at[j, part],
            hid.at[3, part],
            hidf_send.at[group, j],
            hidf_recv.at[group, j],
            device_id={"tp": flip(mine, 3 - j)},
        )

    def give_back(i):
        return pltpu.make_async_remote_copy(
            outb.at[block(i, cap)],
            ret.at[block(i, cap)],
            ret_send.at[i],
            ret_recv.at[i],
            device_id={"ep": flip_by(me, i, ep)},
        )

    tile = length // PARTS

    def head_spread(part, j):
        rows = block(part, tile)
        return pltpu.make_async_remote_copy(
            hm.at[0, rows],
            hm.at[j, rows],
            head_send.at[part, j],
            head_recv.at[part, j],
            device_id={"tp": flip(mine, j)},
        )

    def head_onward(part, j):
        size = tile // 2
        rows = pl.ds(pl.multiple_of(part * tile + (j - 1) * size, size), size)
        return pltpu.make_async_remote_copy(
            hm.at[j, rows],
            hm.at[3, rows],
            hfwd_send.at[part, j],
            hfwd_recv.at[part, j],
            device_id={"tp": flip(mine, 3 - j)},
        )

    def chain(h):
        return pltpu.make_async_remote_copy(
            st_out.at[h],
            st_in.at[h],
            st_send.at[h],
            st_recv.at[h],
            device_id={"ep": me + 1},
        )

    def send_group(group):
        with scope("S"):
            for r in range(per):

                @pl.when(group * per + r > 0)
                def _():
                    dispatch(group * per + r).wait_recv()

        for j in direct:
            spread(group, j).start()

    def relay_group(group):
        if square:
            for j in direct:
                with scope("R"):
                    spread(group, j).wait_recv()
                onward(group, j).start()

    def collect_group(group):
        with scope("C"):
            for j in direct:
                (onward if square else spread)(group, j).wait_recv()

    def relay_share(group):
        if square:
            for j in direct:
                with scope("Q"):
                    share(group, j).wait_recv()
                share_onward(group, j).start()

    def expand(group):
        rows = block(group, span)
        gate = jnp.zeros((span, units), F32)
        up = jnp.zeros((span, units), F32)
        squares = jnp.zeros((span, 1), F32)
        for j in range(tp):
            piece = tok[j, rows, :]
            columns = pl.ds(pl.multiple_of(flip(mine, j) * width, width), width)
            gate += dot(piece, wg_ref[:, columns], ((1,), (1,)))
            up += dot(piece, wu_ref[:, columns], ((1,), (1,)))
            wide = piece.astype(F32)
            squares += jnp.sum(wide * wide, axis=1, keepdims=True)
        inverse = lax.rsqrt(squares / model_width + EPSILON)
        hid[0, rows, :] = (jax.nn.silu(gate * inverse) * (up * inverse)).astype(BF16)
        for j in direct:
            share(group, j).start()

    def contract(group):
        rows = block(group, span)
        with scope("K"):
            for j in direct:
                (share_onward if square else share)(group, j).wait_recv()
        total = jnp.zeros((span, width), F32)
        for j in range(tp):
            at = pl.ds(pl.multiple_of(flip(mine, j) * units, units), units)
            total += dot(hid[j, rows, :], wd_ref[at, :])
        outb[rows, :] = total.astype(BF16)
        for r in range(per):

            @pl.when(group * per + r > 0)
            def _():
                give_back(group * per + r).start()

    for i in range(1, ep):

        @pl.when(jnp.logical_not(held(i)))
        def _():
            dispatch(i).start()

    send_group(0)

    loads[0].wait()
    loads[1].wait()

    def summarise(h, carry):
        keys = k_ref[:, block(h, qk)]
        values = v_ref[:, block(h, vw)]
        log_in = a_ref[pl.ds(h, 1), :]
        top = jnp.max(log_in, axis=1, keepdims=True)
        weighted = keys.astype(F32) * jnp.exp(upright(log_in) - top)
        local[h, 0:qk, :] = dot(weighted.astype(BF16), values, ((0,), (0,)))
        normal = jnp.sum(weighted, axis=0, keepdims=True)
        local[h, qk : qk + 8, 0:qk] = jnp.broadcast_to(normal, (8, qk))
        decay = cum_ref[pl.ds(h, 1), :][:, length - 1 : length]
        local[h, qk + 8 : qk + 16, :] = jnp.broadcast_to(top + decay, (8, vw))
        return carry

    with scope("summarise"):
        lax.fori_loop(0, head_count, summarise, 0)

    @pl.when(me == 0)
    def _():
        st_in[:, 0 : qk + 8, :] = jnp.zeros((head_count, qk + 8, vw), F32)
        st_in[:, qk + 8 : qk + 16, :] = jnp.full((head_count, 8, vw), LOG_FLOOR, F32)

    def carry_on(h, carry):
        @pl.when(me > 0)
        def _():
            with scope("chainwait"):
                chain(h).wait_recv()

        decay = cum_ref[pl.ds(h, 1), :][:, length - 1 : length]
        carried_max = st_in[h, qk + 8 : qk + 9, :] + decay
        own_max = local[h, qk + 8 : qk + 9, :]
        new_max = jnp.maximum(carried_max, own_max)
        keep = jnp.exp(carried_max - new_max)
        add = jnp.exp(own_max - new_max)
        st_out[h, 0:qk, :] = keep * st_in[h, 0:qk, :] + add * local[h, 0:qk, :]
        st_out[h, qk : qk + 8, 0:qk] = (
            keep[:, 0:qk] * st_in[h, qk : qk + 8, 0:qk]
            + add[:, 0:qk] * local[h, qk : qk + 8, 0:qk]
        )
        st_out[h, qk : qk + 8, qk:vw] = jnp.zeros((8, vw - qk), F32)
        st_out[h, qk + 8 : qk + 16, :] = jnp.broadcast_to(new_max, (8, vw))

        @pl.when(me < ep - 1)
        def _():
            chain(h).start()

        return carry

    def heads(h, carry):
        columns = block(h, vw)
        queries = q_ref[:, block(h, qk)]
        keys = k_ref[:, block(h, qk)]
        scale = qk**-0.5
        causal = lax.broadcasted_iota(jnp.int32, (length, length), 1) <= lax.broadcasted_iota(
            jnp.int32, (length, length), 0
        )
        log_in = jnp.where(causal, a_ref[pl.ds(h, 1), :], -jnp.inf)
        prior_max = st_in[h, qk + 8 : qk + 9, 0:1]
        top = jnp.maximum(prior_max, jnp.max(log_in, axis=1, keepdims=True))
        scores = dot(queries, keys, ((1,), (1,))) * scale * jnp.exp(log_in - top)
        carried = jnp.exp(prior_max - top) * scale
        memory = st_in[h, 0:qk, :]
        high = memory.astype(BF16)
        low = (memory - high.astype(F32)).astype(BF16)
        numerator = carried * (dot(queries, high) + dot(queries, low)) + dot(
            scores.astype(BF16), v_ref[:, columns]
        )
        normal = st_in[h, qk : qk + 1, 0:qk]
        denominator = carried * jnp.sum(
            queries.astype(F32) * normal, axis=1, keepdims=True
        ) + jnp.sum(scores, axis=1, keepdims=True)
        floor = jnp.exp(-(upright(cum_ref[pl.ds(h, 1), :]) + top))
        value = numerator / jnp.maximum(jnp.abs(denominator), floor)
        value = value * lax.rsqrt(jnp.mean(value * value, axis=1, keepdims=True) + EPSILON)
        gate = jax.nn.sigmoid(og_ref[:, columns].astype(F32))
        hm[0, :, columns] = (value * gain_ref[:, columns] * gate).astype(BF16)
        return carry

    for at in range(2, 7):
        loads[at].wait()

    def when_between(step, low, high):
        return pl.when((step >= low) & (step <= high))

    quarter = me // (ep // 4)

    def step(k, carry):
        @pl.when(k < GROUPS - 1)
        def _():
            send_group(k + 1)

        @pl.when(k == quarter * (GROUPS // 4))
        def _():
            with scope("chain"):
                lax.fori_loop(0, head_count, carry_on, 0)
            for i in range(2, ep):

                @pl.when(held(i))
                def _():
                    dispatch(i).start()

            with scope("heads"):
                lax.fori_loop(0, head_count, heads, 0)

        @pl.when(k < GROUPS)
        def _():
            relay_group(k)

        @when_between(k, 1, GROUPS)
        def _():
            collect_group(k - 1)
            with scope("expand"):
                expand(k - 1)

        @when_between(k, GROUPS + 1, GROUPS + 2)
        def _():
            for j in direct:
                head_spread(k - GROUPS - 1, j).start()

        @when_between(k, 2, GROUPS + 1)
        def _():
            relay_share(k - 2)

        @pl.when(k >= 3)
        def _():
            contract(k - 3)

        return carry

    lax.fori_loop(0, GROUPS + 3, step, 0)
    for part in range(2, PARTS):
        for j in direct:
            head_spread(part, j).start()
    ret[0:cap, :] = outb[0:cap, :]

    def relay_heads(part):
        if square:
            for j in direct:
                with scope("HR"):
                    head_spread(part, j).wait_recv()
                head_onward(part, j).start()

    loads[7].wait()
    relay_heads(0)

    def combine():
        with scope("retwait"):
            for i in range(1, ep):
                give_back(i).wait_recv()
        places = lax.broadcasted_iota(jnp.int32, (slots.shape[0], tokens), 0)
        total = jnp.zeros((tokens, width), F32)
        for route in range(weight_ref.shape[0]):
            hit = places == slot_row_ref[route : route + 1, :]
            picked = dot(hit.astype(F32).astype(BF16), ret[...], ((0,), (0,)))
            total += picked * upright(weight_ref[route : route + 1, :])
        exp_ref[...] = total.astype(BF16)

    def mix(part, carry):
        @pl.when(part < PARTS - 1)
        def _():
            relay_heads(part + 1)

        @pl.when(part == PARTS - 1)
        def _():
            combine()

        with scope("M"):
            for j in direct:
                (head_onward if square else head_spread)(part, j).wait_recv()
        rows = block(part, tile)
        total = jnp.zeros((tile, width), F32)
        for j in range(tp):
            inputs = pl.ds(pl.multiple_of(flip(mine, j) * width, width), width)
            total += dot(hm[j, rows, :], wm_ref[inputs, :])
        mix_ref[rows, :] = total.astype(BF16)
        return carry

    lax.fori_loop(0, PARTS, mix, 0)

    for i in range(1, ep):
        dispatch(i).wait_send()
        give_back(i).wait_send()

    def finish_group(group, carry):
        for j in direct:
            spread(group, j).wait_send()
            share(group, j).wait_send()
            if square:
                onward(group, j).wait_send()
                share_onward(group, j).wait_send()
        return carry

    lax.fori_loop(0, GROUPS, finish_group, 0)

    def finish_part(part, carry):
        for j in direct:
            head_spread(part, j).wait_send()
            if square:
                head_onward(part, j).wait_send()
        return carry

    lax.fori_loop(0, PARTS, finish_part, 0)
    for h in range(head_count):

        @pl.when(me < ep - 1)
        def _():
            chain(h).wait_send()


def body(
    query_rows,
    key_rows,
    value_rows,
    in_gate,
    forget_gate,
    out_gate,
    head_gain,
    mix_weight,
    expert_input,
    routes,
    route_weight,
    gate_weight,
    up_weight,
    down_weight,
):
    ep, tp = lax.axis_size("ep"), lax.axis_size("tp")
    head_count, length = in_gate.shape
    token_count, fanout = routes.shape
    width = expert_input.shape[1]
    units = gate_weight.shape[1]
    capacity = 2 * token_count * fanout // ep
    slot_count = ep * capacity
    qk = query_rows.shape[1] // head_count
    vw = value_rows.shape[1] // head_count

    earlier = jnp.tril(jnp.ones((length, length), F32))
    cumulative = jnp.einsum(
        "hs,ts->ht", jax.nn.log_sigmoid(forget_gate), earlier, precision=lax.Precision.HIGHEST
    )
    shifted = in_gate - cumulative

    me = lax.axis_index("ep")
    turned = routes ^ me
    experts = jnp.arange(ep, dtype=jnp.int32)
    named = turned[:, :, None] == experts
    any_named = jnp.any(named, axis=1)
    before = jnp.dot(
        jnp.tril(jnp.ones((token_count, token_count), BF16), -1),
        any_named.astype(BF16),
        preferred_element_type=F32,
    ).astype(jnp.int32)
    places = experts * capacity + before
    slot_row = jnp.sum(jnp.where(named, places[:, None, :], 0), axis=2).T

    vmem = pl.BlockSpec(memory_space=pltpu.VMEM)
    anywhere = pl.BlockSpec(memory_space=pl.ANY)
    dma = pltpu.SemaphoreType.DMA
    gate_local, up_local, down_local = gate_weight[0], up_weight[0], down_weight[0]
    big = (query_rows, key_rows, value_rows, out_gate, gate_local, up_local, down_local, mix_weight)
    state = (head_count, qk + PAD, vw)
    return pl.pallas_call(
        functools.partial(kernel, ep, tp, head_count, mix_weight.shape[0]),
        out_shape=(
            jax.ShapeDtypeStruct((length, width), BF16),
            jax.ShapeDtypeStruct((token_count, width), BF16),
        ),
        in_specs=[vmem] * 6 + [anywhere] * 8,
        out_specs=(vmem, vmem),
        scratch_shapes=[pltpu.VMEM(array.shape, array.dtype) for array in big]
        + [
            pltpu.VMEM((slot_count, width), BF16),
            pltpu.VMEM((tp, slot_count, width), BF16),
            pltpu.VMEM((tp, slot_count, units), BF16),
            pltpu.VMEM((slot_count, width), BF16),
            pltpu.VMEM((slot_count, width), BF16),
            pltpu.VMEM((tp, length, width), BF16),
            pltpu.VMEM(state, F32),
            pltpu.VMEM(state, F32),
            pltpu.VMEM(state, F32),
            dma((8,)),
            dma((ep,)),
            dma((ep,)),
            dma((GROUPS, tp)),
            dma((GROUPS, tp)),
            dma((GROUPS, 4)),
            dma((GROUPS, 4)),
            dma((GROUPS, tp)),
            dma((GROUPS, tp)),
            dma((GROUPS, 4)),
            dma((GROUPS, 4)),
            dma((ep,)),
            dma((ep,)),
            dma((PARTS, tp)),
            dma((PARTS, tp)),
            dma((PARTS, 4)),
            dma((PARTS, 4)),
            dma((head_count,)),
            dma((head_count,)),
        ],
        compiler_params=pltpu.CompilerParams(
            collective_id=0, has_side_effects=True, vmem_limit_bytes=64000 * 1024
        ),
    )(
        expert_input,
        slot_row,
        route_weight.T,
        shifted,
        cumulative,
        head_gain[None, :],
        *big,
    )


def solution(mesh):
    in_specs = (
        P("ep", "tp"),
        P("ep", "tp"),
        P("ep", "tp"),
        P("tp", "ep"),
        P("tp", "ep"),
        P("ep", "tp"),
        P("tp"),
        P(None, "tp"),
        P("ep", "tp"),
        P("ep", None),
        P("ep", None),
        P("ep", "tp", None),
        P("ep", "tp", None),
        P("ep", None, "tp"),
    )
    out_specs = (P("ep", "tp"), P("ep", "tp"))
    return jax.shard_map(body, mesh=mesh, in_specs=in_specs, out_specs=out_specs, check_vma=False)
```

time: 174 us -> 152 us (0.87)
  the two profiles are of different devices: /device:TPU:8 before, /device:TPU:25 now
where the time goes in v1:
time: 152 us
  Pallas kernels  144 us (95%)
  local copies, waits for them, and re-layouts  3.12 us (2%)
  matrix products  2.21 us (1%)
    pallas_call x1, Pallas kernels, body(): pl.pallas_call(functools.partial(kernel, ep, tp, head_count, mix_weight.s...  144 us
    unnamed x4, local copies, waits for them, and re-layouts  3.12 us

profile of v1, /device:TPU:25, one launch (start us, length us, event | category | flops | bytes accessed | tf_op | source)
XLA Modules:
  0.0 151.8 jit_solution(6961910581524908044)
XLA Ops:
  0.7 0.7 broadcast_xor_fusion
  1.4 0.2 fusion
  1.6 0.6 select_reduce_fusion
  2.2 2.0 %fusion.25 = (f32[4,512]{1,0:T(4,128)}, f32[4,512]{1,0:T(4,128)}) fusion(f32[4,512]{1,0:T(4,128)} %param.17, f32[4,512]{1,0:T(4,128)} %param.18), kind=kOutput, calls=%fused_computation.32 | convolution fusion | flops 13125632 | bytes 32768 | tf_op jit(solution)/shard_map/hs,ts->ht/dot_general | solution.py:569
  4.2 144.5 %shard_map.149 = (bf16[512,1024]{1,0:T(8,128)(2,1)}, bf16[256,1024]{1,0:T(8,128)(2,1)}) custom-call(bf16[256,1024]{1,0:T(8,128)(2,1)} %x_ref.1, s32[2,256]{1,0:T(2,128)} %bitcast.10, f32[2,256]{1,0:T(2,128)} %bitcast.12, f32[4,512]{1,0:T(4,128)} %get-tuple-element.2.a_ref, f32[4,512]{1,0:T(4,128)} %get-tuple-element.3.cum_ref, f32[1,1024]{1,0:T(1,128)} %bitcast.11, ...), custom_call_target="tpu_custom_call" | custom-call | tf_op jit(solution)/shard_map/pallas_call | solution.py:593
  148.7 0.0 copy-start
  148.7 2.3 %copy.20 = bf16[512,1024]{1,0:T(8,128)(2,1)} copy(bf16[512,1024]{1,0:T(8,128)(2,1)} %get-tuple-element.6) | data formatting | bytes 2097152
  151.0 0.0 copy-done
  151.0 0.8 copy.21
  (3 shorter events, 0.0 us)
Async XLA Ops:
  148.7 2.3 %copy-start = (bf16[256,1024]{1,0:T(8,128)(2,1)S(1)}, bf16[256,1024]{1,0:T(8,128)(2,1)}, u32[]{:S(2)}) copy-start(bf16[256,1024]{1,0:T(8,128)(2,1)} %get-tuple-element.7) | copy-start | bytes 1572868

commit v2 on v1

--- a/solution.py
+++ b/solution.py
@@ -11,7 +11,6 @@
 LOG_FLOOR = -1e30
 F32 = jnp.float32
 BF16 = jnp.bfloat16
-GROUPS = 8
 PARTS = 4
 PAD = 16
 
@@ -55,10 +54,10 @@
     head_count,
     model_width,
     x_ref,
-    slot_row_ref,
+    routes_ref,
     weight_ref,
-    a_ref,
-    cum_ref,
+    in_ref,
+    forget_ref,
     gain_ref,
     q_hbm,
     k_hbm,
@@ -68,8 +67,8 @@
     wu_hbm,
     wd_hbm,
     wm_hbm,
-    mix_ref,
-    exp_ref,
+    mix_hbm,
+    exp_hbm,
     q_ref,
     k_ref,
     v_ref,
@@ -78,7 +77,17 @@
     wu_ref,
     wd_ref,
     wm_ref,
-    slots,
+    mix_ref,
+    exp_ref,
+    a_ref,
+    cum_ref,
+    slot_row_ref,
+    pos_ref,
+    named_ref,
+    rall,
+    full,
+    zraw,
+    afull,
     tok,
     hid,
     outb,
@@ -88,8 +97,22 @@
     st_in,
     st_out,
     load_sem,
-    disp_send,
-    disp_recv,
+    out_sem,
+    route_send,
+    route_recv,
+    own_send,
+    own_recv,
+    ownf_send,
+    ownf_recv,
+    part_send,
+    part_recv,
+    up_send,
+    down_send,
+    side_send,
+    z_recv,
+    a_send,
+    a_side,
+    a_recv,
     tok_send,
     tok_recv,
     fwd_send,
@@ -109,9 +132,7 @@
 ):
     me = lax.axis_index("ep")
     mine = lax.axis_index("tp")
-    cap = slots.shape[0] // ep
-    span = slots.shape[0] // GROUPS
-    per = ep // GROUPS
+    span = outb.shape[0] // ep
     width = x_ref.shape[1]
     length = q_ref.shape[0]
     qk = q_ref.shape[1] // head_count
@@ -149,32 +170,104 @@
     def block(at, size):
         return pl.ds(pl.multiple_of(at * size, size), size)
 
-    def pick(part, carry):
-        size = slots.shape[0] // 4
-        rows = part * size + lax.broadcasted_iota(jnp.int32, (size, tokens), 0)
-        hit = (rows == slot_row_ref[0:1, :]) | (rows == slot_row_ref[1:2, :])
-        chosen = dot(hit.astype(F32).astype(BF16), x_ref[...]).astype(BF16)
-        slots[block(part, size), :] = chosen
-        return carry
-
-    with scope("pick"):
-        lax.fori_loop(0, 4, pick, 0)
-    tok[0, 0:cap, :] = slots[0:cap, :]
+    def route_copy(i):
+        return pltpu.make_async_remote_copy(
+            named_ref,
+            rall.at[me],
+            route_send.at[i],
+            route_recv.at[i],
+            device_id={"ep": flip(me, i)},
+        )
+
+    def route_arrival(i):
+        source = flip(me, i)
+        return pltpu.make_async_remote_copy(
+            named_ref,
+            rall.at[source],
+            route_send.at[i],
+            route_recv.at[i],
+            device_id={"ep": source},
+        )
+
+    def own_spread(j, part):
+        rows = pl.ds(part * (tokens // 2), tokens // 2)
+        return pltpu.make_async_remote_copy(
+            x_ref.at[rows],
+            full.at[0, j, rows],
+            own_send.at[j, part],
+            own_recv.at[j, part],
+            device_id={"tp": flip(mine, j)},
+        )
+
+    def own_onward(j):
+        size = tokens // 2
+        part = pl.ds((j - 1) * size, size)
+        return pltpu.make_async_remote_copy(
+            full.at[0, j, part],
+            full.at[0, 3, part],
+            ownf_send.at[j],
+            ownf_recv.at[j],
+            device_id={"tp": flip(mine, 3 - j)},
+        )
+
+    def to_partner(j):
+        return pltpu.make_async_remote_copy(
+            full.at[0, j] if j else x_ref,
+            full.at[1, j],
+            part_send.at[j],
+            part_recv.at[j],
+            device_id={"ep": flip(me, 1)},
+        )
+
+    def z_copy(source, target, sems, own=False):
+        return pltpu.make_async_remote_copy(
+            x_ref if own else zraw.at[source],
+            zraw.at[source],
+            sems.at[source],
+            z_recv.at[source],
+            device_id={"ep": target},
+        )
+
+    parity = me % 2
+    last = ep - 1
+    spare = flip(me - parity, 2)
+
+    def wide_copy(j, target, sems, start_full):
+        return pltpu.make_async_remote_copy(
+            full.at[0, j] if start_full else afull.at[j],
+            afull.at[j],
+            sems.at[j],
+            a_recv.at[j],
+            device_id={"ep": target},
+        )
+
+    def index_of(place):
+        middle = jnp.where(place == 2, 3 - parity, place + 1)
+        return jnp.where(place < 2, place, jnp.where(place == last, 2 + parity, middle))
+
+    routes = routes_ref[...].astype(F32)
+    named_ref[0:2, :] = routes
+    named_ref[2:8, :] = jnp.full((6, tokens), -1.0, F32)
+    full[0, 0] = x_ref[...]
     with scope("barrier"):
         pl.semaphore_wait(barrier, ep - 1 + tp - 1)
 
-    def dispatch(i):
-        return pltpu.make_async_remote_copy(
-            slots.at[block(i, cap)],
-            tok.at[0, block(i, cap)],
-            disp_send.at[i],
-            disp_recv.at[i],
-            device_id={"ep": flip_by(me, i, ep)},
-        )
-
-    def held(i):
-        ahead = (me % 2 == 1) & (flip(me, i) > me)
-        return ahead if i >= ep // 2 else ahead & (me < 2)
+    for step in range(2):
+        for j in direct:
+            own_spread(j, (j - 1 + step) % 2).start()
+    for i in range(1, ep):
+        route_copy(i).start()
+
+    @pl.when(me < ep - 2)
+    def _():
+        z_copy(me, me + 2, up_send, own=True).start()
+
+    @pl.when(me >= 2)
+    def _():
+        z_copy(me, me - 2, down_send, own=True).start()
+
+    to_partner(0).start()
+    rall[me] = named_ref[...]
 
     def spread(group, j):
         return pltpu.make_async_remote_copy(
@@ -216,10 +309,10 @@
             device_id={"tp": flip(mine, 3 - j)},
         )
 
-    def give_back(i):
-        return pltpu.make_async_remote_copy(
-            outb.at[block(i, cap)],
-            ret.at[block(i, cap)],
+    def give_back(place, i):
+        return pltpu.make_async_remote_copy(
+            outb.at[block(place, span)],
+            ret.at[block(i, span)],
             ret_send.at[i],
             ret_recv.at[i],
             device_id={"ep": flip_by(me, i, ep)},
@@ -257,16 +350,96 @@
             device_id={"ep": me + 1},
         )
 
+    def pass_along(distance):
+        below, above = me - 2 * distance, me + 2 * distance
+
+        @pl.when(below >= 0)
+        def _():
+            with scope("F"):
+                z_copy(below, me, up_send).wait_recv()
+
+            @pl.when(me < ep - 2)
+            def _():
+                z_copy(below, me + 2, up_send).start()
+
+            z_copy(below, flip(me, 1), side_send).start()
+
+        @pl.when(above < ep)
+        def _():
+            with scope("F"):
+                z_copy(above, me, down_send).wait_recv()
+
+            @pl.when(me >= 2)
+            def _():
+                z_copy(above, me - 2, down_send).start()
+
+            z_copy(above, flip(me, 1), side_send).start()
+
+    def choose(source, rows):
+        places = lax.broadcasted_iota(jnp.int32, (span, tokens), 0).astype(F32)
+        hit = places == pos_ref[pl.ds(source, 1), :]
+        return dot(hit.astype(F32).astype(BF16), rows).astype(BF16)
+
     def send_group(group):
-        with scope("S"):
-            for r in range(per):
-
-                @pl.when(group * per + r > 0)
-                def _():
-                    dispatch(group * per + r).wait_recv()
-
+        index = index_of(group)
+        source = flip_by(me, index, ep)
+
+        @pl.when(group == 2)
+        def _():
+            pass_along(1)
+
+        @pl.when((group > 2) & (index % 2 == 0))
+        def _():
+            pass_along(index // 2)
+
+        @pl.when(index % 2 == 1)
+        def _():
+            with scope("S"):
+                z_copy(source, me, side_send).wait_recv()
+
+        tok[0, block(group, span), :] = choose(source, zraw[source])
         for j in direct:
             spread(group, j).start()
+
+    def relay_own():
+        for j in direct:
+            with scope("O"):
+                own_spread(j, (j - 1) % 2).wait_recv()
+            if square:
+                own_onward(j).start()
+        for j in direct:
+            with scope("O"):
+                own_spread(j, j % 2).wait_recv()
+            to_partner(j).start()
+
+    def take_own():
+        if square:
+            with scope("O"):
+                for j in direct:
+                    own_onward(j).wait_recv()
+            to_partner(3).start()
+        for j in range(tp):
+            tok[j, 0:span, :] = choose(me, full[0, j])
+
+    def take_wide():
+        @pl.when(parity == 1)
+        def _():
+            with scope("A"):
+                z_copy(spare, me, side_send).wait_recv()
+                for j in range(1, tp):
+                    wide_copy(j, me, a_side, False).wait_recv()
+
+        rows = block(last, span)
+        tok[0, rows, :] = choose(spare, zraw[spare])
+        for j in range(1, tp):
+            tok[j, rows, :] = choose(spare, afull[j])
+
+    def take_partner():
+        with scope("P"):
+            for j in range(tp):
+                to_partner(j).wait_recv()
+        for j in range(tp):
+            tok[j, span : 2 * span, :] = choose(flip(me, 1), full[1, j])
 
     def relay_group(group):
         if square:
@@ -314,19 +487,38 @@
             at = pl.ds(pl.multiple_of(flip(mine, j) * units, units), units)
             total += dot(hid[j, rows, :], wd_ref[at, :])
         outb[rows, :] = total.astype(BF16)
-        for r in range(per):
-
-            @pl.when(group * per + r > 0)
-            def _():
-                give_back(group * per + r).start()
-
-    for i in range(1, ep):
-
-        @pl.when(jnp.logical_not(held(i)))
-        def _():
-            dispatch(i).start()
-
-    send_group(0)
+
+        @pl.when(group > 0)
+        def _():
+            give_back(group, index_of(group)).start()
+
+    forget = forget_ref[...]
+    decay_log = jnp.minimum(forget, 0.0) - jnp.log1p(jnp.exp(-jnp.abs(forget)))
+    head_part = decay_log.astype(BF16)
+    rest = decay_log - head_part.astype(F32)
+    mid_part = rest.astype(BF16)
+    low_part = (rest - mid_part.astype(F32)).astype(BF16)
+    upper = lax.broadcasted_iota(jnp.int32, (length, length), 0) <= lax.broadcasted_iota(
+        jnp.int32, (length, length), 1
+    )
+    upper = upper.astype(F32).astype(BF16)
+    cumulative = dot(head_part, upper) + dot(mid_part, upper) + dot(low_part, upper)
+    cum_ref[...] = cumulative
+    a_ref[...] = in_ref[...] - cumulative
+
+    strict = lax.broadcasted_iota(jnp.int32, (tokens, tokens), 0) < lax.broadcasted_iota(
+        jnp.int32, (tokens, tokens), 1
+    )
+    strict = strict.astype(F32).astype(BF16)
+    order = lax.broadcasted_iota(jnp.int32, (ep, tokens), 0)
+    experts = (order ^ me).astype(F32)
+    one = jnp.ones((ep, tokens), F32)
+    none = jnp.zeros((ep, tokens), F32)
+    first = jnp.where(experts == routes[0:1, :], one, none)
+    second = jnp.where(experts == routes[1:2, :], one, none)
+    places = (order * span).astype(F32) + dot((first + second).astype(BF16), strict)
+    slot_row_ref[0:1, :] = jnp.sum(first * places, axis=0, keepdims=True)
+    slot_row_ref[1:2, :] = jnp.sum(second * places, axis=0, keepdims=True)
 
     loads[0].wait()
     loads[1].wait()
@@ -411,45 +603,81 @@
     for at in range(2, 7):
         loads[at].wait()
 
+    with scope("routes"):
+        for i in range(1, ep):
+            route_arrival(i).wait_recv()
+    wanted = jnp.zeros((ep, tokens), F32) + me.astype(F32)
+    named = (rall[:, 0, :] == wanted) | (rall[:, 1, :] == wanted)
+    ahead = dot(jnp.where(named, one, none).astype(BF16), strict)
+    pos_ref[...] = jnp.where(named, ahead, -one)
+
     def when_between(step, low, high):
         return pl.when((step >= low) & (step <= high))
 
     quarter = me // (ep // 4)
 
     def step(k, carry):
-        @pl.when(k < GROUPS - 1)
+        @when_between(k, 1, ep - 3)
         def _():
             send_group(k + 1)
 
-        @pl.when(k == quarter * (GROUPS // 4))
+        @pl.when((k == 3) & (parity == 0))
+        def _():
+            for j in range(1, tp):
+                wide_copy(j, flip(me, 2), a_send, True).start()
+
+        @pl.when((k == last - 1) & (parity == 0))
+        def _():
+            for j in range(1, tp):
+                with scope("A"):
+                    wide_copy(j, me, a_send, False).wait_recv()
+                wide_copy(j, flip(me, 1), a_side, False).start()
+
+        @pl.when(k == quarter * (ep // 4))
         def _():
             with scope("chain"):
                 lax.fori_loop(0, head_count, carry_on, 0)
-            for i in range(2, ep):
-
-                @pl.when(held(i))
-                def _():
-                    dispatch(i).start()
-
+
+        @pl.when(k == quarter * (ep // 4) + 1)
+        def _():
             with scope("heads"):
                 lax.fori_loop(0, head_count, heads, 0)
 
-        @pl.when(k < GROUPS)
+        @pl.when(k == 0)
+        def _():
+            relay_own()
+
+        @when_between(k, 2, last - 1)
         def _():
             relay_group(k)
 
-        @when_between(k, 1, GROUPS)
+        @pl.when(k == 1)
+        def _():
+            take_own()
+
+        @pl.when(k == 2)
+        def _():
+            take_partner()
+
+        @when_between(k, 3, last)
         def _():
             collect_group(k - 1)
+
+        @pl.when(k == ep)
+        def _():
+            take_wide()
+
+        @when_between(k, 1, ep)
+        def _():
             with scope("expand"):
                 expand(k - 1)
 
-        @when_between(k, GROUPS + 1, GROUPS + 2)
+        @when_between(k, ep + 1, ep + 2)
         def _():
             for j in direct:
-                head_spread(k - GROUPS - 1, j).start()
-
-        @when_between(k, 2, GROUPS + 1)
+                head_spread(k - ep - 1, j).start()
+
+        @when_between(k, 2, ep + 1)
         def _():
             relay_share(k - 2)
 
@@ -459,11 +687,11 @@
 
         return carry
 
-    lax.fori_loop(0, GROUPS + 3, step, 0)
+    lax.fori_loop(0, ep + 3, step, 0)
     for part in range(2, PARTS):
         for j in direct:
             head_spread(part, j).start()
-    ret[0:cap, :] = outb[0:cap, :]
+    ret[0:span, :] = outb[0:span, :]
 
     def relay_heads(part):
         if square:
@@ -475,22 +703,96 @@
     loads[7].wait()
     relay_heads(0)
 
+    def mix_out(part):
+        rows = block(part, tile)
+        return pltpu.make_async_copy(mix_ref.at[rows], mix_hbm.at[rows], out_sem.at[part])
+
+    exp_out = pltpu.make_async_copy(exp_ref, exp_hbm, out_sem.at[PARTS])
+
+    def settle():
+        for i in range(1, ep):
+            route_copy(i).wait_send()
+        for j in direct:
+            own_spread(j, 0).wait_send()
+            own_spread(j, 1).wait_send()
+            if square:
+                own_onward(j).wait_send()
+        for j in range(tp):
+            to_partner(j).wait_send()
+
+        @pl.when(parity == 0)
+        def _():
+            for j in range(1, tp):
+                wide_copy(j, flip(me, 2), a_send, True).wait_send()
+                wide_copy(j, flip(me, 1), a_side, False).wait_send()
+
+        for distance in range(ep // 2):
+            below, above = me - 2 * distance, me + 2 * distance
+            own = distance == 0
+
+            @pl.when((below >= 0) & (me < ep - 2))
+            def _():
+                z_copy(below, me + 2, up_send, own).wait_send()
+
+            @pl.when((above < ep) & (me >= 2))
+            def _():
+                z_copy(above, me - 2, down_send, own).wait_send()
+
+            if not own:
+
+                @pl.when(below >= 0)
+                def _():
+                    z_copy(below, flip(me, 1), side_send).wait_send()
+
+                @pl.when(above < ep)
+                def _():
+                    z_copy(above, flip(me, 1), side_send).wait_send()
+
+
+        def finish_group(group, carry):
+            for j in direct:
+                share(group, j).wait_send()
+                if square:
+                    share_onward(group, j).wait_send()
+
+            @pl.when((group >= 2) & (group < last))
+            def _():
+                for j in direct:
+                    spread(group, j).wait_send()
+                    if square:
+                        onward(group, j).wait_send()
+
+            return carry
+
+        lax.fori_loop(0, ep, finish_group, 0)
+
+        for h in range(head_count):
+
+            @pl.when(me < ep - 1)
+            def _():
+                chain(h).wait_send()
+
     def combine():
         with scope("retwait"):
             for i in range(1, ep):
-                give_back(i).wait_recv()
-        places = lax.broadcasted_iota(jnp.int32, (slots.shape[0], tokens), 0)
+                give_back(i, i).wait_recv()
+        places = lax.broadcasted_iota(jnp.int32, (ret.shape[0], tokens), 0).astype(F32)
         total = jnp.zeros((tokens, width), F32)
         for route in range(weight_ref.shape[0]):
             hit = places == slot_row_ref[route : route + 1, :]
             picked = dot(hit.astype(F32).astype(BF16), ret[...], ((0,), (0,)))
             total += picked * upright(weight_ref[route : route + 1, :])
         exp_ref[...] = total.astype(BF16)
+        exp_out.start()
 
     def mix(part, carry):
         @pl.when(part < PARTS - 1)
         def _():
             relay_heads(part + 1)
+
+        @pl.when(part == 0)
+        def _():
+            settle()
 
         @pl.when(part == PARTS - 1)
         def _():
@@ -505,38 +807,26 @@
             inputs = pl.ds(pl.multiple_of(flip(mine, j) * width, width), width)
             total += dot(hm[j, rows, :], wm_ref[inputs, :])
         mix_ref[rows, :] = total.astype(BF16)
+        mix_out(part).start()
         return carry
 
     lax.fori_loop(0, PARTS, mix, 0)
 
-    for i in range(1, ep):
-        dispatch(i).wait_send()
-        give_back(i).wait_send()
-
-    def finish_group(group, carry):
-        for j in direct:
-            spread(group, j).wait_send()
-            share(group, j).wait_send()
-            if square:
-                onward(group, j).wait_send()
-                share_onward(group, j).wait_send()
-        return carry
-
-    lax.fori_loop(0, GROUPS, finish_group, 0)
+    with scope("fin1"):
+        for i in range(1, ep):
+            give_back(i, i).wait_send()
 
     def finish_part(part, carry):
+        mix_out(part).wait()
         for j in direct:
             head_spread(part, j).wait_send()
             if square:
                 head_onward(part, j).wait_send()
         return carry
 
-    lax.fori_loop(0, PARTS, finish_part, 0)
-    for h in range(head_count):
-
-        @pl.when(me < ep - 1)
-        def _():
-            chain(h).wait_send()
+    with scope("fin2"):
+        lax.fori_loop(0, PARTS, finish_part, 0)
+        exp_out.wait()
 
 
 def body(
@@ -565,25 +855,6 @@
     qk = query_rows.shape[1] // head_count
     vw = value_rows.shape[1] // head_count
 
-    earlier = jnp.tril(jnp.ones((length, length), F32))
-    cumulative = jnp.einsum(
-        "hs,ts->ht", jax.nn.log_sigmoid(forget_gate), earlier, precision=lax.Precision.HIGHEST
-    )
-    shifted = in_gate - cumulative
-
-    me = lax.axis_index("ep")
-    turned = routes ^ me
-    experts = jnp.arange(ep, dtype=jnp.int32)
-    named = turned[:, :, None] == experts
-    any_named = jnp.any(named, axis=1)
-    before = jnp.dot(
-        jnp.tril(jnp.ones((token_count, token_count), BF16), -1),
-        any_named.astype(BF16),
-        preferred_element_type=F32,
-    ).astype(jnp.int32)
-    places = experts * capacity + before
-    slot_row = jnp.sum(jnp.where(named, places[:, None, :], 0), axis=2).T
-
     vmem = pl.BlockSpec(memory_space=pltpu.VMEM)
     anywhere = pl.BlockSpec(memory_space=pl.ANY)
     dma = pltpu.SemaphoreType.DMA
@@ -597,10 +868,20 @@
             jax.ShapeDtypeStruct((token_count, width), BF16),
         ),
         in_specs=[vmem] * 6 + [anywhere] * 8,
-        out_specs=(vmem, vmem),
+        out_specs=(anywhere, anywhere),
         scratch_shapes=[pltpu.VMEM(array.shape, array.dtype) for array in big]
         + [
-            pltpu.VMEM((slot_count, width), BF16),
+            pltpu.VMEM((length, width), BF16),
+            pltpu.VMEM((token_count, width), BF16),
+            pltpu.VMEM((head_count, length), F32),
+            pltpu.VMEM((head_count, length), F32),
+            pltpu.VMEM((fanout, token_count), F32),
+            pltpu.VMEM((ep, token_count), F32),
+            pltpu.VMEM((8, token_count), F32),
+            pltpu.VMEM((ep, 8, token_count), F32),
+            pltpu.VMEM((2, tp, token_count, width), BF16),
+            pltpu.VMEM((ep, token_count, width), BF16),
+            pltpu.VMEM((tp, token_count, width), BF16),
             pltpu.VMEM((tp, slot_count, width), BF16),
             pltpu.VMEM((tp, slot_count, units), BF16),
             pltpu.VMEM((slot_count, width), BF16),
@@ -610,16 +891,30 @@
             pltpu.VMEM(state, F32),
             pltpu.VMEM(state, F32),
             dma((8,)),
+            dma((PARTS + 1,)),
             dma((ep,)),
             dma((ep,)),
-            dma((GROUPS, tp)),
-            dma((GROUPS, tp)),
-            dma((GROUPS, 4)),
-            dma((GROUPS, 4)),
-            dma((GROUPS, tp)),
-            dma((GROUPS, tp)),
-            dma((GROUPS, 4)),
-            dma((GROUPS, 4)),
+            dma((tp, 2)),
+            dma((tp, 2)),
+            dma((4,)),
+            dma((4,)),
+            dma((tp,)),
+            dma((tp,)),
+            dma((ep,)),
+            dma((ep,)),
+            dma((ep,)),
+            dma((ep,)),
+            dma((tp,)),
+            dma((tp,)),
+            dma((tp,)),
+            dma((ep, tp)),
+            dma((ep, tp)),
+            dma((ep, 4)),
+            dma((ep, 4)),
+            dma((ep, tp)),
+            dma((ep, tp)),
+            dma((ep, 4)),
+            dma((ep, 4)),
             dma((ep,)),
             dma((ep,)),
             dma((PARTS, tp)),
@@ -634,10 +929,10 @@
         ),
     )(
         expert_input,
-        slot_row,
+        routes.T,
         route_weight.T,
-        shifted,
-        cumulative,
+        in_gate,
+        forget_gate,
         head_gain[None, :],
         *big,
     )

time: 152 us -> 133 us (0.88)
  the two profiles are of different devices: /device:TPU:25 before, /device:TPU:0 now
where the time goes in v2:
time: 133 us
  Pallas kernels  129 us (97%)
  local copies, waits for them, and re-layouts  3.12 us (2%)
    pallas_call x1, Pallas kernels, body(): pl.pallas_call(functools.partial(kernel, ep, tp, head_count, mix_weight.s...  129 us
    unnamed x4, local copies, waits for them, and re-layouts  3.12 us

profile of v2, /device:TPU:0, one launch (start us, length us, event | category | flops | bytes accessed | tf_op | source)
XLA Modules:
  0.0 132.7 jit_solution(1513130882539534701)
XLA Ops:
  0.6 129.0 %shard_map.149 = (bf16[512,1024]{1,0:T(8,128)(2,1)}, bf16[256,1024]{1,0:T(8,128)(2,1)}) custom-call(bf16[256,1024]{1,0:T(8,128)(2,1)} %x_ref.1, s32[2,256]{1,0:T(2,128)} %bitcast.10, f32[2,256]{1,0:T(2,128)} %bitcast.11, f32[4,512]{1,0:T(4,128)} %in_ref.1, f32[4,512]{1,0:T(4,128)} %forget_ref.1, f32[1,1024]{1,0:T(1,128)} %bitcast.9, bf16[512,512]{1,0:T(8,128)(2,1)} %q_hbm.1, ...), custom_call_target="tpu_custom_call" | custom-call | tf_op jit(solution)/shard_map/pallas_call | solution.py:864
  129.6 0.0 copy-start
  129.6 2.3 %copy.18 = bf16[512,1024]{1,0:T(8,128)(2,1)} copy(bf16[512,1024]{1,0:T(8,128)(2,1)} %get-tuple-element.4) | data formatting | bytes 2097152
  131.9 0.0 copy-done
  131.9 0.8 copy.19
Async XLA Ops:
  129.6 2.3 %copy-start = (bf16[256,1024]{1,0:T(8,128)(2,1)S(1)}, bf16[256,1024]{1,0:T(8,128)(2,1)}, u32[]{:S(2)}) copy-start(bf16[256,1024]{1,0:T(8,128)(2,1)} %get-tuple-element.5) | copy-start | bytes 1572868

commit v3 on v2

--- a/solution.py
+++ b/solution.py
@@ -53,12 +53,12 @@
     tp,
     head_count,
     model_width,
-    x_ref,
-    routes_ref,
-    weight_ref,
-    in_ref,
-    forget_ref,
-    gain_ref,
+    x_hbm,
+    routes_hbm,
+    weight_hbm,
+    in_hbm,
+    forget_hbm,
+    gain_hbm,
     q_hbm,
     k_hbm,
     v_hbm,
@@ -67,8 +67,14 @@
     wu_hbm,
     wd_hbm,
     wm_hbm,
-    mix_hbm,
-    exp_hbm,
+    mix_ref,
+    exp_ref,
+    x_ref,
+    routes_ref,
+    weight_ref,
+    in_ref,
+    forget_ref,
+    gain_ref,
     q_ref,
     k_ref,
     v_ref,
@@ -77,8 +83,6 @@
     wu_ref,
     wd_ref,
     wm_ref,
-    mix_ref,
-    exp_ref,
     a_ref,
     cum_ref,
     slot_row_ref,
@@ -96,38 +100,27 @@
     local,
     st_in,
     st_out,
+    partial,
     load_sem,
-    out_sem,
-    route_send,
+    sent,
     route_recv,
-    own_send,
     own_recv,
-    ownf_send,
     ownf_recv,
-    part_send,
     part_recv,
     up_send,
     down_send,
     side_send,
     z_recv,
-    a_send,
-    a_side,
     a_recv,
-    tok_send,
     tok_recv,
-    fwd_send,
+    tok_rest,
     fwd_recv,
-    hid_send,
     hid_recv,
-    hidf_send,
     hidf_recv,
-    ret_send,
     ret_recv,
-    head_send,
     head_recv,
-    hfwd_send,
+    head_rest,
     hfwd_recv,
-    st_send,
     st_recv,
 ):
     me = lax.axis_index("ep")
@@ -145,6 +138,12 @@
         pltpu.make_async_copy(source, target, load_sem.at[at])
         for at, (source, target) in enumerate(
             [
+                (x_hbm, x_ref),
+                (routes_hbm, routes_ref),
+                (forget_hbm, forget_ref),
+                (in_hbm, in_ref),
+                (weight_hbm, weight_ref),
+                (gain_hbm, gain_ref),
                 (k_hbm, k_ref),
                 (v_hbm, v_ref),
                 (q_hbm, q_ref),
@@ -156,37 +155,30 @@
             ]
         )
     ]
-    for load in loads:
-        load.start()
-
     barrier = pltpu.get_barrier_semaphore()
     for i in range(1, ep):
         pl.semaphore_signal(barrier, inc=1, device_id={"ep": flip(me, i)})
     for j in range(1, tp):
         pl.semaphore_signal(barrier, inc=1, device_id={"tp": flip(mine, j)})
 
+    for load in loads:
+        load.start()
+
     tokens = x_ref.shape[0]
 
     def block(at, size):
         return pl.ds(pl.multiple_of(at * size, size), size)
 
+    def settled(ref, sem):
+        return pltpu.make_async_remote_copy(ref, ref, sem, sem, device_id={"tp": flip(mine, 1)})
+
     def route_copy(i):
         return pltpu.make_async_remote_copy(
             named_ref,
             rall.at[me],
-            route_send.at[i],
-            route_recv.at[i],
+            sent.at[0],
+            route_recv.at[0],
             device_id={"ep": flip(me, i)},
-        )
-
-    def route_arrival(i):
-        source = flip(me, i)
-        return pltpu.make_async_remote_copy(
-            named_ref,
-            rall.at[source],
-            route_send.at[i],
-            route_recv.at[i],
-            device_id={"ep": source},
         )
 
     def own_spread(j, part):
@@ -194,8 +186,8 @@
         return pltpu.make_async_remote_copy(
             x_ref.at[rows],
             full.at[0, j, rows],
-            own_send.at[j, part],
-            own_recv.at[j, part],
+            sent.at[1],
+            own_recv.at[j - 1, part],
             device_id={"tp": flip(mine, j)},
         )
 
@@ -205,8 +197,8 @@
         return pltpu.make_async_remote_copy(
             full.at[0, j, part],
             full.at[0, 3, part],
-            ownf_send.at[j],
-            ownf_recv.at[j],
+            sent.at[2],
+            ownf_recv.at[j - 1],
             device_id={"tp": flip(mine, 3 - j)},
         )
 
@@ -214,7 +206,7 @@
         return pltpu.make_async_remote_copy(
             full.at[0, j] if j else x_ref,
             full.at[1, j],
-            part_send.at[j],
+            sent.at[3],
             part_recv.at[j],
             device_id={"ep": flip(me, 1)},
         )
@@ -232,11 +224,11 @@
     last = ep - 1
     spare = flip(me - parity, 2)
 
-    def wide_copy(j, target, sems, start_full):
+    def wide_copy(j, target, start_full):
         return pltpu.make_async_remote_copy(
             full.at[0, j] if start_full else afull.at[j],
             afull.at[j],
-            sems.at[j],
+            sent.at[4 if start_full else 5],
             a_recv.at[j],
             device_id={"ep": target},
         )
@@ -245,6 +237,8 @@
         middle = jnp.where(place == 2, 3 - parity, place + 1)
         return jnp.where(place < 2, place, jnp.where(place == last, 2 + parity, middle))
 
+    loads[0].wait()
+    loads[1].wait()
     routes = routes_ref[...].astype(F32)
     named_ref[0:2, :] = routes
     named_ref[2:8, :] = jnp.full((6, tokens), -1.0, F32)
@@ -269,24 +263,28 @@
     to_partner(0).start()
     rall[me] = named_ref[...]
 
-    def spread(group, j):
-        return pltpu.make_async_remote_copy(
-            tok.at[0, block(group, span)],
-            tok.at[j, block(group, span)],
-            tok_send.at[group, j],
-            tok_recv.at[group, j],
+    half = span // 2
+
+    def piece(start, at, size):
+        return pl.ds(pl.multiple_of(start + at * size, size), size)
+
+    def spread(group, j, turn):
+        rows = piece(group * span, (j - 1 + turn) % 2, half)
+        return pltpu.make_async_remote_copy(
+            tok.at[0, rows],
+            tok.at[j, rows],
+            sent.at[6],
+            tok_rest.at[group - 2] if turn else tok_recv.at[group - 2, j - 1],
             device_id={"tp": flip(mine, j)},
         )
 
-    half = span // 2
-
     def onward(group, j):
-        part = pl.ds(pl.multiple_of(group * span + (j - 1) * half, half), half)
+        part = piece(group * span, j - 1, half)
         return pltpu.make_async_remote_copy(
             tok.at[j, part],
             tok.at[3, part],
-            fwd_send.at[group, j],
-            fwd_recv.at[group, j],
+            sent.at[7],
+            fwd_recv.at[group - 2],
             device_id={"tp": flip(mine, 3 - j)},
         )
 
@@ -294,18 +292,18 @@
         return pltpu.make_async_remote_copy(
             hid.at[0, block(group, span)],
             hid.at[j, block(group, span)],
-            hid_send.at[group, j],
-            hid_recv.at[group, j],
+            sent.at[8],
+            hid_recv.at[group, j - 1],
             device_id={"tp": flip(mine, j)},
         )
 
     def share_onward(group, j):
-        part = pl.ds(pl.multiple_of(group * span + (j - 1) * half, half), half)
+        part = piece(group * span, j - 1, half)
         return pltpu.make_async_remote_copy(
             hid.at[j, part],
             hid.at[3, part],
-            hidf_send.at[group, j],
-            hidf_recv.at[group, j],
+            sent.at[9],
+            hidf_recv.at[group],
             device_id={"tp": flip(mine, 3 - j)},
         )
 
@@ -313,31 +311,31 @@
         return pltpu.make_async_remote_copy(
             outb.at[block(place, span)],
             ret.at[block(i, span)],
-            ret_send.at[i],
-            ret_recv.at[i],
+            sent.at[10],
+            ret_recv.at[0],
             device_id={"ep": flip_by(me, i, ep)},
         )
 
     tile = length // PARTS
-
-    def head_spread(part, j):
-        rows = block(part, tile)
+    tile_half = tile // 2
+
+    def head_spread(part, j, turn):
+        rows = piece(part * tile, (j - 1 + turn) % 2, tile_half)
         return pltpu.make_async_remote_copy(
             hm.at[0, rows],
             hm.at[j, rows],
-            head_send.at[part, j],
-            head_recv.at[part, j],
+            sent.at[11],
+            head_rest.at[part] if turn else head_recv.at[part, j - 1],
             device_id={"tp": flip(mine, j)},
         )
 
     def head_onward(part, j):
-        size = tile // 2
-        rows = pl.ds(pl.multiple_of(part * tile + (j - 1) * size, size), size)
+        rows = piece(part * tile, j - 1, tile_half)
         return pltpu.make_async_remote_copy(
             hm.at[j, rows],
             hm.at[3, rows],
-            hfwd_send.at[part, j],
-            hfwd_recv.at[part, j],
+            sent.at[12],
+            hfwd_recv.at[part],
             device_id={"tp": flip(mine, 3 - j)},
         )
 
@@ -345,10 +343,12 @@
         return pltpu.make_async_remote_copy(
             st_out.at[h],
             st_in.at[h],
-            st_send.at[h],
+            sent.at[13],
             st_recv.at[h],
             device_id={"ep": me + 1},
         )
+
+    many = pl.ds(0, len(direct))
 
     def pass_along(distance):
         below, above = me - 2 * distance, me + 2 * distance
@@ -399,7 +399,7 @@
 
         tok[0, block(group, span), :] = choose(source, zraw[source])
         for j in direct:
-            spread(group, j).start()
+            spread(group, j, 0).start()
 
     def relay_own():
         for j in direct:
@@ -427,7 +427,7 @@
             with scope("A"):
                 z_copy(spare, me, side_send).wait_recv()
                 for j in range(1, tp):
-                    wide_copy(j, me, a_side, False).wait_recv()
+                    wide_copy(j, me, False).wait_recv()
 
         rows = block(last, span)
         tok[0, rows, :] = choose(spare, zraw[spare])
@@ -445,13 +445,17 @@
         if square:
             for j in direct:
                 with scope("R"):
-                    spread(group, j).wait_recv()
+                    spread(group, j, 0).wait_recv()
                 onward(group, j).start()
 
     def collect_group(group):
         with scope("C"):
-            for j in direct:
-                (onward if square else spread)(group, j).wait_recv()
+            if square:
+                settled(tok.at[3, block(group, span)], fwd_recv.at[group - 2]).wait_recv()
+            else:
+                for j in direct:
+                    spread(group, j, 0).wait_recv()
+            settled(tok.at[many, piece(0, 0, half)], tok_rest.at[group - 2]).wait_recv()
 
     def relay_share(group):
         if square:
@@ -480,8 +484,11 @@
     def contract(group):
         rows = block(group, span)
         with scope("K"):
-            for j in direct:
-                (share_onward if square else share)(group, j).wait_recv()
+            if square:
+                settled(hid.at[3, block(group, span)], hidf_recv.at[group]).wait_recv()
+            else:
+                for j in direct:
+                    share(group, j).wait_recv()
         total = jnp.zeros((span, width), F32)
         for j in range(tp):
             at = pl.ds(pl.multiple_of(flip(mine, j) * units, units), units)
@@ -492,6 +499,8 @@
         def _():
             give_back(group, index_of(group)).start()
 
+    for at in range(2, 6):
+        loads[at].wait()
     forget = forget_ref[...]
     decay_log = jnp.minimum(forget, 0.0) - jnp.log1p(jnp.exp(-jnp.abs(forget)))
     head_part = decay_log.astype(BF16)
@@ -520,8 +529,8 @@
     slot_row_ref[0:1, :] = jnp.sum(first * places, axis=0, keepdims=True)
     slot_row_ref[1:2, :] = jnp.sum(second * places, axis=0, keepdims=True)
 
-    loads[0].wait()
-    loads[1].wait()
+    loads[6].wait()
+    loads[7].wait()
 
     def summarise(h, carry):
         keys = k_ref[:, block(h, qk)]
@@ -600,12 +609,11 @@
         hm[0, :, columns] = (value * gain_ref[:, columns] * gate).astype(BF16)
         return carry
 
-    for at in range(2, 7):
+    for at in range(8, 14):
         loads[at].wait()
 
     with scope("routes"):
-        for i in range(1, ep):
-            route_arrival(i).wait_recv()
+        settled(rall.at[pl.ds(0, ep - 1)], route_recv.at[0]).wait_recv()
     wanted = jnp.zeros((ep, tokens), F32) + me.astype(F32)
     named = (rall[:, 0, :] == wanted) | (rall[:, 1, :] == wanted)
     ahead = dot(jnp.where(named, one, none).astype(BF16), strict)
@@ -615,116 +623,54 @@
         return pl.when((step >= low) & (step <= high))
 
     quarter = me // (ep // 4)
-
-    def step(k, carry):
-        @when_between(k, 1, ep - 3)
-        def _():
-            send_group(k + 1)
-
-        @pl.when((k == 3) & (parity == 0))
-        def _():
-            for j in range(1, tp):
-                wide_copy(j, flip(me, 2), a_send, True).start()
-
-        @pl.when((k == last - 1) & (parity == 0))
-        def _():
-            for j in range(1, tp):
-                with scope("A"):
-                    wide_copy(j, me, a_send, False).wait_recv()
-                wide_copy(j, flip(me, 1), a_side, False).start()
-
-        @pl.when(k == quarter * (ep // 4))
-        def _():
-            with scope("chain"):
-                lax.fori_loop(0, head_count, carry_on, 0)
-
-        @pl.when(k == quarter * (ep // 4) + 1)
-        def _():
-            with scope("heads"):
-                lax.fori_loop(0, head_count, heads, 0)
-
-        @pl.when(k == 0)
-        def _():
-            relay_own()
-
-        @when_between(k, 2, last - 1)
-        def _():
-            relay_group(k)
-
-        @pl.when(k == 1)
+    slot = (quarter + 2 * jnp.minimum(quarter, 1)) * (ep // 8)
+    first_part = last
+
+    def absorb(group, carry):
+        @pl.when(group == 0)
         def _():
             take_own()
 
-        @pl.when(k == 2)
+        @pl.when(group == 1)
         def _():
             take_partner()
 
-        @when_between(k, 3, last)
-        def _():
-            collect_group(k - 1)
-
-        @pl.when(k == ep)
+        @when_between(group, 2, last - 1)
+        def _():
+            collect_group(group)
+
+        @pl.when(group == last)
         def _():
             take_wide()
 
-        @when_between(k, 1, ep)
-        def _():
-            with scope("expand"):
-                expand(k - 1)
-
-        @when_between(k, ep + 1, ep + 2)
-        def _():
-            for j in direct:
-                head_spread(k - ep - 1, j).start()
-
-        @when_between(k, 2, ep + 1)
-        def _():
-            relay_share(k - 2)
-
-        @pl.when(k >= 3)
-        def _():
-            contract(k - 3)
-
+        with scope("expand"):
+            expand(group)
         return carry
 
-    lax.fori_loop(0, ep + 3, step, 0)
-    for part in range(2, PARTS):
-        for j in direct:
-            head_spread(part, j).start()
-    ret[0:span, :] = outb[0:span, :]
+    def pass_share(group, carry):
+        relay_share(group)
+        return carry
+
+    def finish_group(group, carry):
+        contract(group)
+        return carry
 
     def relay_heads(part):
         if square:
             for j in direct:
                 with scope("HR"):
-                    head_spread(part, j).wait_recv()
+                    head_spread(part, j, 0).wait_recv()
                 head_onward(part, j).start()
 
-    loads[7].wait()
-    relay_heads(0)
-
-    def mix_out(part):
-        rows = block(part, tile)
-        return pltpu.make_async_copy(mix_ref.at[rows], mix_hbm.at[rows], out_sem.at[part])
-
-    exp_out = pltpu.make_async_copy(exp_ref, exp_hbm, out_sem.at[PARTS])
-
     def settle():
-        for i in range(1, ep):
-            route_copy(i).wait_send()
-        for j in direct:
-            own_spread(j, 0).wait_send()
-            own_spread(j, 1).wait_send()
-            if square:
-                own_onward(j).wait_send()
-        for j in range(tp):
-            to_partner(j).wait_send()
+        settled(rall.at[pl.ds(0, ep - 1)], sent.at[0]).wait_send()
+        settled(full.at[0, pl.ds(1, len(direct))], sent.at[1]).wait_send()
+        settled(full.at[1], sent.at[3]).wait_send()
 
         @pl.when(parity == 0)
         def _():
-            for j in range(1, tp):
-                wide_copy(j, flip(me, 2), a_send, True).wait_send()
-                wide_copy(j, flip(me, 1), a_side, False).wait_send()
+            settled(afull.at[pl.ds(1, tp - 1)], sent.at[4]).wait_send()
+            settled(afull.at[pl.ds(1, tp - 1)], sent.at[5]).wait_send()
 
         for distance in range(ep // 2):
             below, above = me - 2 * distance, me + 2 * distance
@@ -748,34 +694,23 @@
                 def _():
                     z_copy(above, flip(me, 1), side_send).wait_send()
 
-
-        def finish_group(group, carry):
-            for j in direct:
-                share(group, j).wait_send()
-                if square:
-                    share_onward(group, j).wait_send()
-
-            @pl.when((group >= 2) & (group < last))
-            def _():
-                for j in direct:
-                    spread(group, j).wait_send()
-                    if square:
-                        onward(group, j).wait_send()
-
-            return carry
-
-        lax.fori_loop(0, ep, finish_group, 0)
-
-        for h in range(head_count):
-
-            @pl.when(me < ep - 1)
-            def _():
-                chain(h).wait_send()
+        spread_rows = pl.ds(0, (ep - 3) * span)
+        settled(tok.at[many, spread_rows], sent.at[6]).wait_send()
+        settled(hid.at[many], sent.at[8]).wait_send()
+        if square:
+            settled(full.at[0, 3], sent.at[2]).wait_send()
+            settled(tok.at[0, spread_rows], sent.at[7]).wait_send()
+            settled(hid.at[0], sent.at[9]).wait_send()
+
+        @pl.when(me < ep - 1)
+        def _():
+            settled(st_out, sent.at[13]).wait_send()
 
     def combine():
+        returns = pl.ds(0, (ep - 1) * span)
         with scope("retwait"):
-            for i in range(1, ep):
-                give_back(i, i).wait_recv()
+            settled(ret.at[returns], ret_recv.at[0]).wait_recv()
+        ret[0:span, :] = outb[0:span, :]
         places = lax.broadcasted_iota(jnp.int32, (ret.shape[0], tokens), 0).astype(F32)
         total = jnp.zeros((tokens, width), F32)
         for route in range(weight_ref.shape[0]):
@@ -783,50 +718,114 @@
             picked = dot(hit.astype(F32).astype(BF16), ret[...], ((0,), (0,)))
             total += picked * upright(weight_ref[route : route + 1, :])
         exp_ref[...] = total.astype(BF16)
-        exp_out.start()
-
-    def mix(part, carry):
-        @pl.when(part < PARTS - 1)
-        def _():
-            relay_heads(part + 1)
-
-        @pl.when(part == 0)
+        settled(ret.at[returns], sent.at[10]).wait_send()
+
+    def mix(part):
+        rows = block(part, tile)
+        with scope("M"):
+            if not square:
+                for j in direct:
+                    head_spread(part, j, 0).wait_recv()
+            settled(hm.at[many, piece(0, 0, tile_half)], head_rest.at[part]).wait_recv()
+
+        def share_of(j):
+            inputs = pl.ds(pl.multiple_of(flip(mine, j) * width, width), width)
+            return dot(hm[j, rows, :], wm_ref[inputs, :])
+
+        total = jnp.zeros((tile, width), F32)
+        for j in range(tp - 1):
+            total += share_of(j)
+        partial[...] = total
+        if square:
+            with scope("M2"):
+                settled(hm.at[3, rows], hfwd_recv.at[part]).wait_recv()
+        mix_ref[rows, :] = (partial[...] + share_of(tp - 1)).astype(BF16)
+
+    def step(k, carry):
+        @pl.when(k == slot)
+        def _():
+            with scope("chain"):
+                lax.fori_loop(0, head_count, carry_on, 0)
+            with scope("heads"):
+                lax.fori_loop(0, head_count // 2, heads, 0)
+
+        @pl.when(k == slot + 1)
+        def _():
+            with scope("heads"):
+                lax.fori_loop(head_count // 2, head_count, heads, 0)
+
+        @pl.when(k == 0)
+        def _():
+            relay_own()
+
+        @when_between(k, 2, last + 1)
+        def _():
+            lax.fori_loop(jnp.where(k == 2, 0, k - 1), k, absorb, 0)
+
+        @when_between(k, 2, last - 1)
+        def _():
+            relay_group(k)
+
+        @when_between(k, first_part, first_part + PARTS - 1)
+        def _():
+            relay_heads(k - first_part)
+
+        @when_between(k, 3, last + 2)
+        def _():
+            lax.fori_loop(jnp.where(k == 3, 0, k - 2), k - 1, finish_group, 0)
+
+        @when_between(k, 1, last - 2)
+        def _():
+            send_group(k + 1)
+
+        @when_between(k, first_part - 1, first_part + PARTS - 2)
+        def _():
+            for j in direct:
+                head_spread(k + 1 - first_part, j, 0).start()
+
+        @when_between(k, 2, last + 1)
+        def _():
+            lax.fori_loop(jnp.where(k == 2, 0, k - 1), k, pass_share, 0)
+
+        @when_between(k, 1, last - 2)
+        def _():
+            for j in direct:
+                spread(k + 1, j, 1).start()
+
+        @when_between(k, first_part - 1, first_part + PARTS - 2)
+        def _():
+            for j in direct:
+                head_spread(k + 1 - first_part, j, 1).start()
+
+        @pl.when((k == 2) & (parity == 0))
+        def _():
+            for j in range(1, tp):
+                wide_copy(j, flip(me, 2), True).start()
+
+        @pl.when((k == last - 1) & (parity == 0))
+        def _():
+            for j in range(1, tp):
+                with scope("A"):
+                    wide_copy(j, me, False).wait_recv()
+                wide_copy(j, flip(me, 1), False).start()
+
+        @pl.when(k == first_part + PARTS)
         def _():
             settle()
-
-        @pl.when(part == PARTS - 1)
-        def _():
             combine()
 
-        with scope("M"):
-            for j in direct:
-                (head_onward if square else head_spread)(part, j).wait_recv()
-        rows = block(part, tile)
-        total = jnp.zeros((tile, width), F32)
-        for j in range(tp):
-            inputs = pl.ds(pl.multiple_of(flip(mine, j) * width, width), width)
-            total += dot(hm[j, rows, :], wm_ref[inputs, :])
-        mix_ref[rows, :] = total.astype(BF16)
-        mix_out(part).start()
+        @pl.when(k > first_part)
+        def _():
+            mix(k - first_part - 1)
+
         return carry
 
-    lax.fori_loop(0, PARTS, mix, 0)
-
-    with scope("fin1"):
-        for i in range(1, ep):
-            give_back(i, i).wait_send()
-
-    def finish_part(part, carry):
-        mix_out(part).wait()
-        for j in direct:
-            head_spread(part, j).wait_send()
-            if square:
-                head_onward(part, j).wait_send()
-        return carry
-
-    with scope("fin2"):
-        lax.fori_loop(0, PARTS, finish_part, 0)
-        exp_out.wait()
+    lax.fori_loop(0, first_part + PARTS + 1, step, 0)
+
+    with scope("fin"):
+        settled(hm.at[many], sent.at[11]).wait_send()
+        if square:
+            settled(hm.at[0], sent.at[12]).wait_send()
 
 
 def body(
@@ -859,20 +858,20 @@
     anywhere = pl.BlockSpec(memory_space=pl.ANY)
     dma = pltpu.SemaphoreType.DMA
     gate_local, up_local, down_local = gate_weight[0], up_weight[0], down_weight[0]
+    small = (expert_input, routes.T, route_weight.T, in_gate, forget_gate, head_gain[None, :])
     big = (query_rows, key_rows, value_rows, out_gate, gate_local, up_local, down_local, mix_weight)
     state = (head_count, qk + PAD, vw)
+    direct = 2 if tp == 4 else tp - 1
     return pl.pallas_call(
         functools.partial(kernel, ep, tp, head_count, mix_weight.shape[0]),
         out_shape=(
-            jax.ShapeDtypeStruct((length, width), BF16),
-            jax.ShapeDtypeStruct((token_count, width), BF16),
-        ),
-        in_specs=[vmem] * 6 + [anywhere] * 8,
-        out_specs=(anywhere, anywhere),
-        scratch_shapes=[pltpu.VMEM(array.shape, array.dtype) for array in big]
-        + [
             pltpu.VMEM((length, width), BF16),
             pltpu.VMEM((token_count, width), BF16),
+        ),
+        in_specs=[anywhere] * 14,
+        out_specs=(vmem, vmem),
+        scratch_shapes=[pltpu.VMEM(array.shape, array.dtype) for array in small + big]
+        + [
             pltpu.VMEM((head_count, length), F32),
             pltpu.VMEM((head_count, length), F32),
             pltpu.VMEM((fanout, token_count), F32),
@@ -890,50 +889,34 @@
             pltpu.VMEM(state, F32),
             pltpu.VMEM(state, F32),
             pltpu.VMEM(state, F32),
-            dma((8,)),
-            dma((PARTS + 1,)),
-            dma((ep,)),
-            dma((ep,)),
-            dma((tp, 2)),
-            dma((tp, 2)),
-            dma((4,)),
-            dma((4,)),
-            dma((tp,)),
+            pltpu.VMEM((length // PARTS, width), F32),
+            dma((14,)),
+            dma((14,)),
+            dma((1,)),
+            dma((direct, 2)),
+            dma((2,)),
             dma((tp,)),
             dma((ep,)),
             dma((ep,)),
             dma((ep,)),
             dma((ep,)),
             dma((tp,)),
-            dma((tp,)),
-            dma((tp,)),
-            dma((ep, tp)),
-            dma((ep, tp)),
-            dma((ep, 4)),
-            dma((ep, 4)),
-            dma((ep, tp)),
-            dma((ep, tp)),
-            dma((ep, 4)),
-            dma((ep, 4)),
+            dma((ep - 3, direct)),
+            dma((ep - 3,)),
+            dma((ep - 3,)),
+            dma((ep, direct)),
             dma((ep,)),
-            dma((ep,)),
-            dma((PARTS, tp)),
-            dma((PARTS, tp)),
-            dma((PARTS, 4)),
-            dma((PARTS, 4)),
-            dma((head_count,)),
+            dma((1,)),
+            dma((PARTS, direct)),
+            dma((PARTS,)),
+            dma((PARTS,)),
             dma((head_count,)),
         ],
         compiler_params=pltpu.CompilerParams(
-            collective_id=0, has_side_effects=True, vmem_limit_bytes=64000 * 1024
+            collective_id=0, has_side_effects=True, vmem_limit_bytes=58000 * 1024
         ),
     )(
-        expert_input,
-        routes.T,
-        route_weight.T,
-        in_gate,
-        forget_gate,
-        head_gain[None, :],
+        *small,
         *big,
     )
 

time: 133 us -> 122 us (0.917)
  Pallas kernels: 129 us -> 119 us
  local copies, waits for them, and re-layouts: 3.12 us -> 1.77 us
    pallas_call x1, Pallas kernels: 129 us -> 119 us  [body(): pl.pallas_call(functools.partial(kernel, ep, tp, head_count, mix_weight.s...]
    unnamed x4 -> x2, local copies, waits for them, and re-layouts: 3.12 us -> 1.77 us
where the time goes in v3:
time: 122 us; the launch traced here: 121 us
  Pallas kernels  119 us (98%)
  local copies, waits for them, and re-layouts  1.77 us (1%)
    pallas_call x1, Pallas kernels, body(): pl.pallas_call(functools.partial(kernel, ep, tp, head_count, mix_weight.s...  119 us

profile of v3, /device:TPU:0, one launch (start us, length us, event | category | flops | bytes accessed | tf_op | source)
XLA Modules:
  0.0 121.4 jit_solution(15648341597766936025)
XLA Ops:
  0.6 119.0 %shard_map.149 = (bf16[512,1024]{1,0:T(8,128)(2,1)S(1)}, bf16[256,1024]{1,0:T(8,128)(2,1)S(1)}) custom-call(bf16[256,1024]{1,0:T(8,128)(2,1)} %x_hbm.1, s32[2,256]{1,0:T(2,128)} %bitcast.10, f32[2,256]{1,0:T(2,128)} %bitcast.11, f32[4,512]{1,0:T(4,128)} %in_hbm.1, f32[4,512]{1,0:T(4,128)} %forget_hbm.1, f32[1,1024]{1,0:T(1,128)} %bitcast.9, ...), custom_call_target="tpu_custom_call" | custom-call | tf_op jit(solution)/shard_map/pallas_call | solution.py:865
  119.6 1.0 copy.18
  120.6 0.8 copy.19

commit v4 on v3

--- a/solution.py
+++ b/solution.py
@@ -92,6 +92,7 @@
     full,
     zraw,
     afull,
+    corner,
     tok,
     hid,
     outb,
@@ -107,11 +108,11 @@
     own_recv,
     ownf_recv,
     part_recv,
-    up_send,
-    down_send,
+    z_send,
     side_send,
     z_recv,
     a_recv,
+    b_recv,
     tok_recv,
     tok_rest,
     fwd_recv,
@@ -211,18 +212,39 @@
             device_id={"ep": flip(me, 1)},
         )
 
-    def z_copy(source, target, sems, own=False):
-        return pltpu.make_async_remote_copy(
-            x_ref if own else zraw.at[source],
+    def z_copy(source, target, part):
+        rows = pl.ds(part * (tokens // 2), tokens // 2)
+        return pltpu.make_async_remote_copy(
+            zraw.at[source, rows],
+            zraw.at[source, rows],
+            z_send.at[source, part],
+            z_recv.at[source, part],
+            device_id={"ep": target},
+        )
+
+    def z_own(target, part, sem):
+        rows = pl.ds(part * (tokens // 2), tokens // 2)
+        return pltpu.make_async_remote_copy(
+            x_ref.at[rows],
+            zraw.at[me, rows],
+            sem,
+            z_recv.at[me, part],
+            device_id={"ep": target},
+        )
+
+    def z_side(source, target):
+        return pltpu.make_async_remote_copy(
             zraw.at[source],
-            sems.at[source],
-            z_recv.at[source],
+            zraw.at[source],
+            side_send.at[source],
+            z_recv.at[source, 0],
             device_id={"ep": target},
         )
 
     parity = me % 2
     last = ep - 1
     spare = flip(me - parity, 2)
+    other = spare + 1
 
     def wide_copy(j, target, start_full):
         return pltpu.make_async_remote_copy(
@@ -230,6 +252,15 @@
             afull.at[j],
             sent.at[4 if start_full else 5],
             a_recv.at[j],
+            device_id={"ep": target},
+        )
+
+    def corner_copy(target, start_full):
+        return pltpu.make_async_remote_copy(
+            full.at[0, 3] if start_full else corner,
+            corner,
+            sent.at[14 if start_full else 15],
+            b_recv.at[0],
             device_id={"ep": target},
         )
 
@@ -252,13 +283,15 @@
     for i in range(1, ep):
         route_copy(i).start()
 
-    @pl.when(me < ep - 2)
-    def _():
-        z_copy(me, me + 2, up_send, own=True).start()
-
-    @pl.when(me >= 2)
-    def _():
-        z_copy(me, me - 2, down_send, own=True).start()
+    for part in range(2):
+
+        @pl.when(me < ep - 2)
+        def _():
+            z_own(me + 2, part, sent.at[16]).start()
+
+        @pl.when(me >= 2)
+        def _():
+            z_own(me - 2, part, sent.at[17]).start()
 
     to_partner(0).start()
     rall[me] = named_ref[...]
@@ -350,30 +383,32 @@
 
     many = pl.ds(0, len(direct))
 
-    def pass_along(distance):
+    def pass_along(distance, part):
         below, above = me - 2 * distance, me + 2 * distance
 
         @pl.when(below >= 0)
         def _():
             with scope("F"):
-                z_copy(below, me, up_send).wait_recv()
+                z_copy(below, me, part).wait_recv()
 
             @pl.when(me < ep - 2)
             def _():
-                z_copy(below, me + 2, up_send).start()
-
-            z_copy(below, flip(me, 1), side_send).start()
+                z_copy(below, me + 2, part).start()
+
+            if part:
+                z_side(below, flip(me, 1)).start()
 
         @pl.when(above < ep)
         def _():
             with scope("F"):
-                z_copy(above, me, down_send).wait_recv()
+                z_copy(above, me, part).wait_recv()
 
             @pl.when(me >= 2)
             def _():
-                z_copy(above, me - 2, down_send).start()
-
-            z_copy(above, flip(me, 1), side_send).start()
+                z_copy(above, me - 2, part).start()
+
+            if part:
+                z_side(above, flip(me, 1)).start()
 
     def choose(source, rows):
         places = lax.broadcasted_iota(jnp.int32, (span, tokens), 0).astype(F32)
@@ -386,16 +421,17 @@
 
         @pl.when(group == 2)
         def _():
-            pass_along(1)
+            pass_along(1, 1)
 
         @pl.when((group > 2) & (index % 2 == 0))
         def _():
-            pass_along(index // 2)
+            pass_along(index // 2, 0)
+            pass_along(index // 2, 1)
 
         @pl.when(index % 2 == 1)
         def _():
             with scope("S"):
-                z_copy(source, me, side_send).wait_recv()
+                z_side(source, me).wait_recv()
 
         tok[0, block(group, span), :] = choose(source, zraw[source])
         for j in direct:
@@ -407,6 +443,7 @@
                 own_spread(j, (j - 1) % 2).wait_recv()
             if square:
                 own_onward(j).start()
+        pass_along(1, 0)
         for j in direct:
             with scope("O"):
                 own_spread(j, j % 2).wait_recv()
@@ -425,7 +462,7 @@
         @pl.when(parity == 1)
         def _():
             with scope("A"):
-                z_copy(spare, me, side_send).wait_recv()
+                z_side(spare, me).wait_recv()
                 for j in range(1, tp):
                     wide_copy(j, me, False).wait_recv()
 
@@ -448,10 +485,28 @@
                     spread(group, j, 0).wait_recv()
                 onward(group, j).start()
 
+    def full_relay(group):
+        rows = block(group, span)
+
+        @pl.when(group > 2)
+        def _():
+            settled(tok.at[3, rows], fwd_recv.at[group - 2]).wait_recv()
+
+        @pl.when(group == 2)
+        def _():
+            for j in direct:
+                spread(group, j, 0).wait_recv()
+
+            @pl.when(parity == 0)
+            def _():
+                corner_copy(me, False).wait_recv()
+
+            tok[3, rows, :] = choose(other, corner[...])
+
     def collect_group(group):
         with scope("C"):
             if square:
-                settled(tok.at[3, block(group, span)], fwd_recv.at[group - 2]).wait_recv()
+                full_relay(group)
             else:
                 for j in direct:
                     spread(group, j, 0).wait_recv()
@@ -623,10 +678,27 @@
         return pl.when((step >= low) & (step <= high))
 
     quarter = me // (ep // 4)
-    slot = (quarter + 2 * jnp.minimum(quarter, 1)) * (ep // 8)
+    slot = quarter * (7 - quarter) // 2 * (ep // 8)
     first_part = last
-
-    def absorb(group, carry):
+    early = (1,) if square else direct
+    late = (1 - (me // 2) % 2) * jnp.minimum(me // 2, 1)
+    final = last + 1 + ((me // 2) % 2) * jnp.minimum(me // 4, 1)
+    tardy = late * (1 - parity)
+
+    def turn(n):
+        return jnp.where(n < 2, n, jnp.where(n == last, n, jnp.where(n == last - 1, 2, n + 1)))
+
+    def turns(k):
+        low = jnp.where(k == 2, 0, jnp.where(k == final, last, k - 2))
+        high = jnp.where(k == last, k, k - 1)
+        return low, jnp.where(k == 2, 2, jnp.where(k == final, last + 1, high))
+
+    def busy(k):
+        return (k == 2) | ((k >= 4) & (k <= last)) | (k == final)
+
+    def absorb(n, carry):
+        group = turn(n)
+
         @pl.when(group == 0)
         def _():
             take_own()
@@ -647,12 +719,12 @@
             expand(group)
         return carry
 
-    def pass_share(group, carry):
-        relay_share(group)
+    def pass_share(n, carry):
+        relay_share(turn(n))
         return carry
 
-    def finish_group(group, carry):
-        contract(group)
+    def finish_group(n, carry):
+        contract(turn(n))
         return carry
 
     def relay_heads(part):
@@ -672,34 +744,47 @@
             settled(afull.at[pl.ds(1, tp - 1)], sent.at[4]).wait_send()
             settled(afull.at[pl.ds(1, tp - 1)], sent.at[5]).wait_send()
 
-        for distance in range(ep // 2):
+        @pl.when(me < ep - 2)
+        def _():
+            settled(x_ref, sent.at[16]).wait_send()
+
+        @pl.when(me >= 2)
+        def _():
+            settled(x_ref, sent.at[17]).wait_send()
+
+        for distance in range(1, ep // 2):
             below, above = me - 2 * distance, me + 2 * distance
-            own = distance == 0
-
-            @pl.when((below >= 0) & (me < ep - 2))
+
+            @pl.when(below >= 0)
             def _():
-                z_copy(below, me + 2, up_send, own).wait_send()
-
-            @pl.when((above < ep) & (me >= 2))
+                z_side(below, flip(me, 1)).wait_send()
+
+                @pl.when(me < ep - 2)
+                def _():
+                    for part in range(2):
+                        z_copy(below, me + 2, part).wait_send()
+
+            @pl.when(above < ep)
             def _():
-                z_copy(above, me - 2, down_send, own).wait_send()
-
-            if not own:
-
-                @pl.when(below >= 0)
+                z_side(above, flip(me, 1)).wait_send()
+
+                @pl.when(me >= 2)
                 def _():
-                    z_copy(below, flip(me, 1), side_send).wait_send()
-
-                @pl.when(above < ep)
-                def _():
-                    z_copy(above, flip(me, 1), side_send).wait_send()
+                    for part in range(2):
+                        z_copy(above, me - 2, part).wait_send()
 
         spread_rows = pl.ds(0, (ep - 3) * span)
         settled(tok.at[many, spread_rows], sent.at[6]).wait_send()
         settled(hid.at[many], sent.at[8]).wait_send()
         if square:
             settled(full.at[0, 3], sent.at[2]).wait_send()
-            settled(tok.at[0, spread_rows], sent.at[7]).wait_send()
+            settled(tok.at[0, pl.ds(0, (ep - 4) * span)], sent.at[7]).wait_send()
+
+            @pl.when(parity == 1)
+            def _():
+                settled(corner, sent.at[14]).wait_send()
+                settled(corner, sent.at[15]).wait_send()
+
             settled(hid.at[0], sent.at[9]).wait_send()
 
         @pl.when(me < ep - 1)
@@ -749,7 +834,7 @@
             with scope("heads"):
                 lax.fori_loop(0, head_count // 2, heads, 0)
 
-        @pl.when(k == slot + 1)
+        @pl.when(k == jnp.minimum(slot + 1, last - 1))
         def _():
             with scope("heads"):
                 lax.fori_loop(head_count // 2, head_count, heads, 0)
@@ -758,11 +843,11 @@
         def _():
             relay_own()
 
-        @when_between(k, 2, last + 1)
-        def _():
-            lax.fori_loop(jnp.where(k == 2, 0, k - 1), k, absorb, 0)
-
-        @when_between(k, 2, last - 1)
+        @pl.when(busy(k))
+        def _():
+            lax.fori_loop(*turns(k), absorb, 0)
+
+        @when_between(k, 3 if square else 2, last - 1)
         def _():
             relay_group(k)
 
@@ -770,9 +855,18 @@
         def _():
             relay_heads(k - first_part)
 
-        @when_between(k, 3, last + 2)
-        def _():
-            lax.fori_loop(jnp.where(k == 3, 0, k - 2), k - 1, finish_group, 0)
+        @pl.when(busy(k - 1))
+        def _():
+            lax.fori_loop(*turns(k - 1), finish_group, 0)
+
+        if square:
+
+            @pl.when((k == final - 1) & (parity == 0))
+            def _():
+                for j in (2, 3):
+                    with scope("A3"):
+                        wide_copy(j, me, False).wait_recv()
+                    wide_copy(j, flip(me, 1), False).start()
 
         @when_between(k, 1, last - 2)
         def _():
@@ -783,9 +877,9 @@
             for j in direct:
                 head_spread(k + 1 - first_part, j, 0).start()
 
-        @when_between(k, 2, last + 1)
-        def _():
-            lax.fori_loop(jnp.where(k == 2, 0, k - 1), k, pass_share, 0)
+        @pl.when(busy(k))
+        def _():
+            lax.fori_loop(*turns(k), pass_share, 0)
 
         @when_between(k, 1, last - 2)
         def _():
@@ -799,12 +893,29 @@
 
         @pl.when((k == 2) & (parity == 0))
         def _():
-            for j in range(1, tp):
+            for j in early:
                 wide_copy(j, flip(me, 2), True).start()
 
+        if square:
+
+            @pl.when((k == 2 + 3 * late) & (parity == 0))
+            def _():
+                for j in (2, 3):
+                    wide_copy(j, flip(me, 2), True).start()
+
+            @pl.when((k == 2) & (parity == 1))
+            def _():
+                corner_copy(flip(me, 2), True).start()
+
+            @pl.when((k == last - 1) & (parity == 1))
+            def _():
+                with scope("B"):
+                    corner_copy(me, False).wait_recv()
+                corner_copy(flip(me, 1), False).start()
+
         @pl.when((k == last - 1) & (parity == 0))
         def _():
-            for j in range(1, tp):
+            for j in early:
                 with scope("A"):
                     wide_copy(j, me, False).wait_recv()
                 wide_copy(j, flip(me, 1), False).start()
@@ -812,11 +923,18 @@
         @pl.when(k == first_part + PARTS)
         def _():
             settle()
+
+        @pl.when((k == first_part + PARTS) & (tardy == 0))
+        def _():
             combine()
 
         @pl.when(k > first_part)
         def _():
             mix(k - first_part - 1)
+
+        @pl.when((k == first_part + PARTS) & (tardy == 1))
+        def _():
+            combine()
 
         return carry
 
@@ -881,6 +999,7 @@
             pltpu.VMEM((2, tp, token_count, width), BF16),
             pltpu.VMEM((ep, token_count, width), BF16),
             pltpu.VMEM((tp, token_count, width), BF16),
+            pltpu.VMEM((token_count, width), BF16),
             pltpu.VMEM((tp, slot_count, width), BF16),
             pltpu.VMEM((tp, slot_count, units), BF16),
             pltpu.VMEM((slot_count, width), BF16),
@@ -891,16 +1010,16 @@
             pltpu.VMEM(state, F32),
             pltpu.VMEM((length // PARTS, width), F32),
             dma((14,)),
-            dma((14,)),
+            dma((18,)),
             dma((1,)),
             dma((direct, 2)),
             dma((2,)),
             dma((tp,)),
+            dma((ep, 2)),
             dma((ep,)),
-            dma((ep,)),
-            dma((ep,)),
-            dma((ep,)),
+            dma((ep, 2)),
             dma((tp,)),
+            dma((1,)),
             dma((ep - 3, direct)),
             dma((ep - 3,)),
             dma((ep - 3,)),

time: 122 us -> 120 us (0.984)
  Pallas kernels: 119 us -> 116 us
    pallas_call x1, Pallas kernels: 119 us -> 116 us  [body(): pl.pallas_call(functools.partial(kernel, ep, tp, head_count, mix_weight.s...]
where the time goes in v4:
time: 120 us; the launch traced here: 119 us
  Pallas kernels  116 us (97%)
  local copies, waits for them, and re-layouts  1.77 us (1%)
    pallas_call x1, Pallas kernels, body(): pl.pallas_call(functools.partial(kernel, ep, tp, head_count, mix_weight.s...  116 us

profile of v4, /device:TPU:0, one launch (start us, length us, event | category | flops | bytes accessed | tf_op | source)
XLA Modules:
  0.0 118.7 jit_solution(10369109960901103968)
XLA Ops:
  0.6 116.3 %shard_map.149 = (bf16[512,1024]{1,0:T(8,128)(2,1)S(1)}, bf16[256,1024]{1,0:T(8,128)(2,1)S(1)}) custom-call(bf16[256,1024]{1,0:T(8,128)(2,1)} %x_hbm.1, s32[2,256]{1,0:T(2,128)} %bitcast.10, f32[2,256]{1,0:T(2,128)} %bitcast.11, f32[4,512]{1,0:T(4,128)} %in_hbm.1, f32[4,512]{1,0:T(4,128)} %forget_hbm.1, f32[1,1024]{1,0:T(1,128)} %bitcast.9, ...), custom_call_target="tpu_custom_call" | custom-call | tf_op jit(solution)/shard_map/pallas_call | solution.py:983
  117.0 1.0 copy.18
  117.9 0.8 copy.19

commit v5 on v4

--- a/solution.py
+++ b/solution.py
@@ -843,7 +843,7 @@
         def _():
             relay_own()
 
-        @pl.when(busy(k))
+        @pl.when(busy(k) & (k != last + 2))
         def _():
             lax.fori_loop(*turns(k), absorb, 0)
 
@@ -855,7 +855,11 @@
         def _():
             relay_heads(k - first_part)
 
-        @pl.when(busy(k - 1))
+        @pl.when((k == final) & (k == last + 2))
+        def _():
+            relay_share(last)
+
+        @pl.when(busy(k - 1) & (k != last + 3))
         def _():
             lax.fori_loop(*turns(k - 1), finish_group, 0)
 
@@ -877,7 +881,7 @@
             for j in direct:
                 head_spread(k + 1 - first_part, j, 0).start()
 
-        @pl.when(busy(k))
+        @pl.when(busy(k) & (k != last + 2))
         def _():
             lax.fori_loop(*turns(k), pass_share, 0)
 
@@ -919,6 +923,14 @@
                 with scope("A"):
                     wide_copy(j, me, False).wait_recv()
                 wide_copy(j, flip(me, 1), False).start()
+
+        @pl.when((k == final - 1) & (k == last + 1))
+        def _():
+            absorb(last, 0)
+
+        @pl.when((k == final) & (k == last + 2))
+        def _():
+            contract(last)
 
         @pl.when(k == first_part + PARTS)
         def _():

time: 120 us -> 119 us (level)
  no operation moved by 1% of the time
where the time goes in v5:
time: 119 us
  Pallas kernels  116 us (97%)
  local copies, waits for them, and re-layouts  1.77 us (1%)
    pallas_call x1, Pallas kernels, body(): pl.pallas_call(functools.partial(kernel, ep, tp, head_count, mix_weight.s...  116 us

profile of v5, /device:TPU:0, one launch (start us, length us, event | category | flops | bytes accessed | tf_op | source)
XLA Modules:
  0.0 118.7 jit_solution(1187467258173465807)
XLA Ops:
  0.6 116.3 %shard_map.149 = (bf16[512,1024]{1,0:T(8,128)(2,1)S(1)}, bf16[256,1024]{1,0:T(8,128)(2,1)S(1)}) custom-call(bf16[256,1024]{1,0:T(8,128)(2,1)} %x_hbm.1, s32[2,256]{1,0:T(2,128)} %bitcast.10, f32[2,256]{1,0:T(2,128)} %bitcast.11, f32[4,512]{1,0:T(4,128)} %in_hbm.1, f32[4,512]{1,0:T(4,128)} %forget_hbm.1, f32[1,1024]{1,0:T(1,128)} %bitcast.9, ...), custom_call_target="tpu_custom_call" | custom-call | tf_op jit(solution)/shard_map/pallas_call | solution.py:995
  117.0 1.0 copy.18
  117.9 0.8 copy.19
